TPU v7x, 512 devices: a whole 4x8x8 slice. The times are simulated.
512 devices in a mesh: sp: 64 (over z, y), tp: 8 (over x, core).
Axes of the slice: x: 4, y: 8, z: 8, core: 2. Of those that a mesh axis runs over, the one named last changes fastest.
Arguments:
- tokens: bfloat16 [8192, 2048], P('sp', 'tp'), may hold values from -6 to 6
- pre_gain: float32 [2048], replicated, may hold values from 0.1 to 1.9
- w_query_stick: bfloat16 [2048, 1024], P(None, 'tp'), may hold values from -0.125 to 0.125
- w_key_stick: bfloat16 [2048, 1024], P(None, 'tp'), may hold values from -0.125 to 0.125
- w_value_stick: bfloat16 [2048, 1024], P(None, 'tp'), may hold values from -2 to 2, as said below
- w_query_window: bfloat16 [2048, 1024], P(None, 'tp'), may hold values from -20 to 20, as said below
- w_key_window: bfloat16 [2048, 512], P(None, 'tp'), may hold values from -1 to 1, as said below
- w_value_window: bfloat16 [2048, 512], P(None, 'tp'), may hold values from -2 to 2, as said below
- stick_bias: float32 [16], P('tp'), may hold values from -14 to -3
- sinks: float32 [16], P('tp'), may hold values from 2 to 6
- stick_gain: float32 [1024], P('tp'), may hold values from 0.1 to 1.9
- window_gain: float32 [1024], P('tp'), may hold values from 0.1 to 1.9
- w_out_stick: bfloat16 [1024, 2048], P('tp'), may hold values from -0.125 to 0.125
- w_out_window: bfloat16 [1024, 2048], P('tp'), may hold values from -0.125 to 0.125
- post_gain: float32 [2048], replicated, may hold values from 0.1 to 1.9
Outputs:
- layer_out: bfloat16 [8192, 2048], P(('sp', 'tp'))
Inputs may be any that keep to these rules, and one draw needn't show every extreme that they name: `w_key_window`: key weights of the windowed heads. `w_query_window`: query weights of the windowed heads. `w_value_stick`: value weights of the stick-breaking heads. `w_value_window`: value weights of the windowed heads.
All inputs are finite; a program needn't handle non-finite values.
Results may differ from a plain program's by a relative error of at most 0.018.
Values may be sent and summed in bfloat16 or wider, within the bound.
No kernel may reach another device: no remote copies, remote signals or barrier semaphores. Data moves between devices by JAX's collectives and lax.ppermute only.
A program may use at most 64 MiB of HBM per device.

v0:
```python
import jax
import jax.numpy as jnp
from jax import lax
from jax.sharding import PartitionSpec as P

HEAD_DIM = 64
GROUP = 2
WINDOW = 128
SB_WIDTH = 1024
SW_WIDTH = 1024


epsilon = 1e-06


def laid_out(tiles, dim):
    tiles = jnp.moveaxis(tiles, 0, dim)
    shape = tiles.shape
    return tiles.reshape(*shape[:dim], shape[dim] * shape[dim + 1], *shape[dim + 2 :])


def from_everyone(array, axis):
    size = lax.axis_size(axis)
    return lax.all_to_all(
        jnp.broadcast_to(array[None], (size, *array.shape)), axis, 0, 0, tiled=True
    )


def gathered_copies(array, axis, dim):
    return laid_out(from_everyone(array, axis), dim)


def passed_along(value, axis, steps):
    count = lax.axis_size(axis)
    initial, last = (max(0, -steps), min(count, count - steps))
    return lax.ppermute(value, axis, [(source, source + steps) for source in range(initial, last)])


def over_copies(array, axis):
    return from_everyone(array, axis).sum(axis=0)


def packed_total(arrays, axis):
    flat, at, outs = (jnp.concatenate([a.reshape(-1) for a in arrays]), 0, [])
    subtotal = over_copies(flat, axis)
    for a in arrays:
        outs.append(subtotal[at : at + a.size].reshape(a.shape))
        at += a.size
    return tuple(outs)


def rounded(values):
    return lax.optimization_barrier(values.astype(jnp.bfloat16)).astype(jnp.float32)


def norm_rows(values, gain):
    stats = jnp.mean(values * values, axis=-1, keepdims=True)
    return values * lax.rsqrt(stats + epsilon) * gain


def stick_block(queries, key_pair, head_bias, key_mask, carried):
    result, logsum = carried
    head_count = queries.shape[1]
    key_rows = key_pair[0].reshape(key_pair.shape[1], head_count, HEAD_DIM)
    values = key_pair[1].reshape(key_pair.shape[1], head_count, HEAD_DIM)
    scores = jnp.einsum(
        "thd,shd->hts", queries, key_rows, preferred_element_type=jnp.float32
    ) * HEAD_DIM ** (-0.5)
    scores = scores + head_bias[:, None, None]
    usable = key_mask[None]
    log_keep = jnp.where(usable, jax.nn.log_sigmoid(-scores), 0.0)
    suffix = lax.cumsum(log_keep, axis=2, reverse=True) - log_keep
    stick_weights = jnp.where(
        usable, jnp.exp(jax.nn.log_sigmoid(scores) + suffix + logsum[:, :, None]), 0.0
    )
    stick_weights = stick_weights.astype(jnp.bfloat16)
    result = result + jnp.einsum(
        "hts,shd->htd", stick_weights, values, preferred_element_type=jnp.float32
    )
    logsum = logsum + jnp.sum(log_keep, axis=2)
    return (result, logsum)


def shards(
    tokens,
    pre_gain,
    w_query_stick,
    w_key_stick,
    w_value_stick,
    w_query_window,
    w_key_window,
    w_value_window,
    stick_bias,
    sinks,
    stick_gain,
    window_gain,
    w_out_stick,
    w_out_window,
    post_gain,
):
    gathered = gathered_copies(tokens, "tp", 1)
    normed = norm_rows(gathered.astype(jnp.float32), pre_gain).astype(jnp.bfloat16)

    def project(weight):
        return jnp.dot(normed, weight, preferred_element_type=jnp.float32).astype(jnp.bfloat16)

    tok_rows = normed.shape[0]
    dev_index = lax.axis_index("sp")
    dev_count = lax.axis_size("sp")
    query_stick = project(w_query_stick)
    stick_heads = query_stick.shape[1] // HEAD_DIM
    queries = query_stick.reshape(tok_rows, stick_heads, HEAD_DIM)
    own_pair = jnp.stack([project(w_key_stick), project(w_value_stick)])
    pair_width = own_pair.shape[2]
    positions = jnp.arange(tok_rows, dtype=jnp.int32)
    initial = (
        jnp.zeros((stick_heads, tok_rows, HEAD_DIM), jnp.float32),
        jnp.zeros((stick_heads, tok_rows), jnp.float32),
    )
    collected = own_pair[None]
    for section_index in range(dev_count.bit_length() - 1):
        arrived = passed_along(collected, "sp", 2**section_index)
        collected = jnp.concatenate([arrived, collected], axis=0)
    per_group = min(dev_count, 8)
    group_count = dev_count // per_group
    grouped = collected.reshape(group_count, per_group, 2, tok_rows, pair_width)
    grouped = grouped.transpose(0, 2, 1, 3, 4).reshape(
        group_count, 2, per_group * tok_rows, pair_width
    )
    first_source = dev_index - (dev_count - 1)
    group_starts = (first_source + jnp.arange(group_count, dtype=jnp.int32) * per_group) * tok_rows
    query_pos = dev_index * tok_rows + positions
    span_offs = jnp.arange(per_group * tok_rows, dtype=jnp.int32)

    def visit_group(carried, inputs):
        key_pair, start_pos = inputs
        key_pos = start_pos + span_offs
        key_mask = (key_pos[None, :] >= 0) & (key_pos[None, :] < query_pos[:, None])
        return (stick_block(queries, key_pair, stick_bias, key_mask, carried), None)

    (stick_sum, _), _ = lax.scan(visit_group, initial, (grouped, group_starts), reverse=True)
    stick_out = (
        stick_sum.transpose(1, 0, 2).reshape(tok_rows, stick_heads * HEAD_DIM).astype(jnp.bfloat16)
    )
    query_window = project(w_query_window)
    window_pair = jnp.stack([project(w_key_window), project(w_value_window)])
    kv_heads = window_pair.shape[2] // HEAD_DIM
    previous = passed_along(window_pair, "sp", 1)
    extended = jnp.concatenate([previous, window_pair], axis=1)
    block_count = tok_rows // WINDOW
    extended = extended.reshape(2, block_count + 1, WINDOW, kv_heads, HEAD_DIM)
    banded = jnp.concatenate([extended[:, :-1], extended[:, 1:]], axis=2)
    q_blocks = query_window.reshape(block_count, WINDOW, kv_heads, GROUP, HEAD_DIM)
    logits = jnp.einsum(
        "nqhgd,nchd->nhgqc", q_blocks, banded[0], preferred_element_type=jnp.float32
    ) * HEAD_DIM ** (-0.5)
    query_offs = jnp.arange(WINDOW, dtype=jnp.int32)[:, None]
    key_offs = jnp.arange(2 * WINDOW, dtype=jnp.int32)[None, :]
    distance = query_offs + WINDOW - key_offs
    key_pos = (
        dev_index * tok_rows
        + jnp.arange(block_count, dtype=jnp.int32)[:, None] * WINDOW
        - WINDOW
        + key_offs
    )
    usable = ((distance >= 0) & (distance < WINDOW))[None] & (key_pos >= 0)[:, None, :]
    logits = jnp.where(usable[:, None, None], logits, -jnp.inf)
    sink_logit = sinks.reshape(kv_heads, GROUP)[None, :, :, None, None]
    row_top = jnp.maximum(jnp.max(logits, axis=-1, keepdims=True), sink_logit)
    weights_exp = jnp.exp(logits - row_top)
    normalizer = jnp.sum(weights_exp, axis=-1, keepdims=True) + jnp.exp(sink_logit - row_top)
    window_weights = (weights_exp / normalizer).astype(jnp.bfloat16)
    window_sum = jnp.einsum(
        "nhgqc,nchd->nqhgd", window_weights, banded[1], preferred_element_type=jnp.float32
    )
    window_out = window_sum.reshape(tok_rows, query_window.shape[1]).astype(jnp.bfloat16)
    stick_float = stick_out.astype(jnp.float32)
    window_float = window_out.astype(jnp.float32)
    squares = packed_total(
        (jnp.sum(stick_float * stick_float, axis=1), jnp.sum(window_float * window_float, axis=1)),
        "tp",
    )
    stick_normed = (
        stick_float * lax.rsqrt(squares[0][:, None] / SB_WIDTH + epsilon) * stick_gain
    ).astype(jnp.bfloat16)
    window_normed = (
        window_float * lax.rsqrt(squares[1][:, None] / SW_WIDTH + epsilon) * window_gain
    ).astype(jnp.bfloat16)
    total = jnp.dot(stick_normed, w_out_stick, preferred_element_type=jnp.float32)
    combined = lax.psum_scatter(
        (total + jnp.dot(window_normed, w_out_window, preferred_element_type=jnp.float32)).astype(
            jnp.bfloat16
        ),
        "tp",
        scatter_dimension=0,
        tiled=True,
    ).astype(jnp.float32)
    combined = rounded(combined)
    return norm_rows(combined, post_gain).astype(jnp.bfloat16)


def solution(mesh):
    in_specs = (
        P("sp", "tp"),
        P(),
        P(None, "tp"),
        P(None, "tp"),
        P(None, "tp"),
        P(None, "tp"),
        P(None, "tp"),
        P(None, "tp"),
        P("tp"),
        P("tp"),
        P("tp"),
        P("tp"),
        P("tp", None),
        P("tp", None),
        P(),
    )
    out_specs = P(("sp", "tp"), None)
    return jax.shard_map(shards, mesh=mesh, in_specs=in_specs, out_specs=out_specs, check_vma=False)
```

profile of v0, /device:TPU:1, one launch (start us, length us, event | category | flops | bytes accessed | tf_op | source)
XLA Modules:
  0.0 460.6 jit_solution(8751095200928946585)
XLA Ops:
  7.7 18.6 %all_to_all.11 = bf16[8,128,256]{1,2,0:T(8,128)(2,1)S(1)} all-to-all(bf16[8,128,256]{1,2,0:T(8,128)(2,1)S(1)} %broadcast_in_dim.51), channel_id=1, replica_groups=mesh['sp'=64,'tp'=8] {'tp'}, dimensions={0} | all-to-all | bytes 1048576 | tf_op jit(solution)/shard_map/all_to_all | solution.py:24
  31.9 3.0 collective-permute-start.1
  34.9 1.9 collective-permute-done.1
  36.9 12.4 %collective-permute-start.2 = (bf16[4,2,128,128]{3,2,1,0:T(8,128)(2,1)S(1)}, bf16[4,2,128,128]{3,2,1,0:T(8,128)(2,1)S(1)}, u32[]{:S(2)}, u32[]{:S(2)}) collective-permute-start(bf16[4,2,128,128]{3,2,1,0:T(8,128)(2,1)S(1)} %pad_maximum_fusion.1), channel_id=1, source_target_pairs={{0,32},{8,40},{16,48},{24,56},{32,64},{40,72},{48,80},{56,88},{64,... | collective-permute-start | bytes 786440 | tf_op jit(solution)/shard_map/ppermute | solution.py:36
  49.3 10.9 %collective-permute-done.2 = bf16[4,2,128,128]{3,2,1,0:T(8,128)(2,1)S(1)} collective-permute-done((bf16[4,2,128,128]{3,2,1,0:T(8,128)(2,1)S(1)}, bf16[4,2,128,128]{3,2,1,0:T(8,128)(2,1)S(1)}, u32[]{:S(2)}, u32[]{:S(2)}) %collective-permute-start.2) | collective-permute-done | bytes 262176 | tf_op jit(solution)/shard_map/ppermute | solution.py:36
  60.3 5.3 %collective-permute-start.3 = (bf16[8,2,128,128]{3,2,1,0:T(8,128)(2,1)S(1)}, bf16[8,2,128,128]{3,2,1,0:T(8,128)(2,1)S(1)}, u32[]{:S(2)}, u32[]{:S(2)}) collective-permute-start(bf16[8,2,128,128]{3,2,1,0:T(8,128)(2,1)S(1)} %pad_maximum_fusion), channel_id=1, source_target_pairs={{0,64},{8,72},{16,80},{24,88},{32,96},{40,104},{48,112},{56,120},{... | collective-permute-start | bytes 1572872 | tf_op jit(solution)/shard_map/ppermute | solution.py:36
  65.6 10.1 %collective-permute-done.3 = bf16[8,2,128,128]{3,2,1,0:T(8,128)(2,1)S(1)} collective-permute-done((bf16[8,2,128,128]{3,2,1,0:T(8,128)(2,1)S(1)}, bf16[8,2,128,128]{3,2,1,0:T(8,128)(2,1)S(1)}, u32[]{:S(2)}, u32[]{:S(2)}) %collective-permute-start.3) | collective-permute-done | bytes 524320 | tf_op jit(solution)/shard_map/ppermute | solution.py:36
  79.2 5.9 %collective-permute-start.4 = (bf16[16,2,128,128]{3,2,1,0:T(8,128)(2,1)}, bf16[16,2,128,128]{3,2,1,0:T(8,128)(2,1)S(1)}, u32[]{:S(2)}, u32[]{:S(2)}) collective-permute-start(bf16[16,2,128,128]{3,2,1,0:T(8,128)(2,1)} %constant_dynamic-update-slice_fusion), channel_id=1, source_target_pairs={{0,128},{8,136},{16,144},{24,152},{32,160},{40,168},{48,176},{56,1... | collective-permute-start | bytes 3145736 | tf_op jit(solution)/shard_map/ppermute | solution.py:36
  88.1 17.8 %collective-permute-done.4 = bf16[16,2,128,128]{3,2,1,0:T(8,128)(2,1)S(1)} collective-permute-done((bf16[16,2,128,128]{3,2,1,0:T(8,128)(2,1)}, bf16[16,2,128,128]{3,2,1,0:T(8,128)(2,1)S(1)}, u32[]{:S(2)}, u32[]{:S(2)}) %collective-permute-start.4) | collective-permute-done | bytes 1048608 | tf_op jit(solution)/shard_map/ppermute | solution.py:36
  110.4 39.2 %collective-permute-start.5 = (bf16[32,2,128,128]{3,2,1,0:T(8,128)(2,1)}, bf16[32,2,128,128]{3,2,1,0:T(8,128)(2,1)}, u32[]{:S(2)}, u32[]{:S(2)}) collective-permute-start(bf16[32,2,128,128]{3,2,1,0:T(8,128)(2,1)} %constant_dynamic-update-slice_fusion.5), channel_id=1, source_target_pairs={{0,256},{8,264},{16,272},{24,280},{32,288},{40,296},{48,304},{56,3... | collective-permute-start | bytes 6291464 | tf_op jit(solution)/shard_map/ppermute | solution.py:36
  152.7 38.8 %collective-permute-done.5 = bf16[32,2,128,128]{3,2,1,0:T(8,128)(2,1)} collective-permute-done((bf16[32,2,128,128]{3,2,1,0:T(8,128)(2,1)}, bf16[32,2,128,128]{3,2,1,0:T(8,128)(2,1)}, u32[]{:S(2)}, u32[]{:S(2)}) %collective-permute-start.5) | collective-permute-done | bytes 2097184 | tf_op jit(solution)/shard_map/ppermute | solution.py:36
  191.5 3.2 constant_dynamic-update-slice_fusion.17
  199.2 6.7 %copy.43 = bf16[8,2,8,128,128]{3,2,4,1,0:T(8,128)(2,1)} copy(bf16[8,2,8,128,128]{4,3,1,2,0:T(8,128)(2,1)} %bitcast.6) | data formatting | bytes 8388608 | tf_op jit(solution)/shard_map/transpose | solution.py:127
  205.9 7.3 %reshape.312 = bf16[8,2,1024,128]{2,3,1,0:T(8,128)(2,1)} reshape(bf16[8,2,8,128,128]{3,2,4,1,0:T(8,128)(2,1)} %copy.43) | data formatting | bytes 8388608 | tf_op jit(solution)/shard_map/reshape | solution.py:127
  213.3 71.4 %while.17 = (s32[]{:T(128)}, f32[2,128,64]{1,2,0:T(8,128)S(1)}, f32[2,128]{1,0:T(2,128)S(1)}, s32[8]{0:T(128)S(1)}, bf16[8,2,1024,128]{2,3,1,0:T(8,128)(2,1)}, /...) while((s32[]{:T(128)}, f32[2,128,64]{1,2,0:T(8,128)S(1)}, ...), condition=%wide.region_5.6_spmd.clone, body=%wide.region_1.5_spmd.clone.sunk | while | flops 109366400 | bytes 13740244 | solution.py:141
  217.5 2.5 fusion.80
  220.4 1.5 fusion.82
  226.5 2.5 fusion.80
  229.4 1.5 fusion.82
  235.4 2.5 fusion.80
  238.3 1.5 fusion.82
  244.3 2.5 fusion.80
  247.2 1.5 fusion.82
  253.2 2.5 fusion.80
  256.1 1.5 fusion.82
  262.2 2.5 fusion.80
  271.1 2.5 fusion.80
  280.0 2.5 fusion.80
  284.7 10.2 %all_to_all.12 = f32[8,1,256]{2,1,0:T(1,128)S(1)} all-to-all(f32[8,1,256]{2,1,0:T(1,128)S(1)} %broadcast_in_dim.81), channel_id=1, replica_groups=mesh['sp'=64,'tp'=8] {'tp'}, dimensions={0} | all-to-all | bytes 16384 | tf_op jit(solution)/shard_map/all_to_all | solution.py:24
  295.5 2.2 fusion.17
  297.6 153.5 %reduce-scatter.2.cloned.1.call-done = bf16[16,2048]{1,0:T(8,128)(2,1)} async-done(((bf16[128,2048]{1,0:T(8,128)(2,1)}), bf16[16,2048]{1,0:T(8,128)(2,1)}) %reduce-scatter.2.cloned.1.call-update) | async-done | bytes 65552 | tf_op jit(solution)/shard_map/reduce_scatter | solution.py:190
  452.2 1.6 fusion.30
  (197 shorter events, 69.7 us)
Async XLA Ops:
  6.5 288.6 %copy-start = (bf16[128,2048]{1,0:T(8,128)(2,1)S(1)}, bf16[128,2048]{1,0:T(8,128)(2,1)}, u32[]{:S(2)}) copy-start(bf16[128,2048]{1,0:T(8,128)(2,1)} %param.29) | copy-start | bytes 1572868
  6.5 22.4 %copy-start.1 = (bf16[2048,128]{1,0:T(8,128)(2,1)S(1)}, bf16[2048,128]{1,0:T(8,128)(2,1)}, u32[]{:S(2)}) copy-start(bf16[2048,128]{1,0:T(8,128)(2,1)} %param.20) | copy-start | bytes 1572868
  6.5 444.6 %reduce-scatter.2.cloned.1.call-start = ((), (), s32[]{:S(2)}) async-start(), calls=%async_computation.3 | async-start | bytes 589824 | tf_op jit(solution)/shard_map/reduce_scatter | solution.py:190
  26.2 59.1 %copy-start.3 = (bf16[2048,64]{0,1:T(8,128)(2,1)S(1)}, bf16[2048,64]{0,1:T(8,128)(2,1)}, u32[]{:S(2)}) copy-start(bf16[2048,64]{0,1:T(8,128)(2,1)} %param.23) | copy-start | bytes 786436
  29.3 2.6 collective-permute-start
  31.9 4.9 %collective-permute-start.1 = (bf16[2,2,128,128]{3,2,1,0:T(8,128)(2,1)S(1)}, bf16[2,2,128,128]{3,2,1,0:T(8,128)(2,1)S(1)}, u32[]{:S(2)}, u32[]{:S(2)}) collective-permute-start(bf16[2,2,128,128]{3,2,1,0:T(8,128)(2,1)S(1)} %pad_maximum_fusion.2), channel_id=1, source_target_pairs={{0,16},{8,24},{16,32},{24,40},{32,48},{40,56},{48,64},{56,72},{64,... | collective-permute-start | bytes 393224 | tf_op jit(solution)/shard_map/ppermute | solution.py:36
  36.9 23.4 %collective-permute-start.2 = (bf16[4,2,128,128]{3,2,1,0:T(8,128)(2,1)S(1)}, bf16[4,2,128,128]{3,2,1,0:T(8,128)(2,1)S(1)}, u32[]{:S(2)}, u32[]{:S(2)}) collective-permute-start(bf16[4,2,128,128]{3,2,1,0:T(8,128)(2,1)S(1)} %pad_maximum_fusion.1), channel_id=1, source_target_pairs={{0,32},{8,40},{16,48},{24,56},{32,64},{40,72},{48,80},{56,88},{64,... | collective-permute-start | bytes 786440 | tf_op jit(solution)/shard_map/ppermute | solution.py:36
  60.3 15.4 %collective-permute-start.3 = (bf16[8,2,128,128]{3,2,1,0:T(8,128)(2,1)S(1)}, bf16[8,2,128,128]{3,2,1,0:T(8,128)(2,1)S(1)}, u32[]{:S(2)}, u32[]{:S(2)}) collective-permute-start(bf16[8,2,128,128]{3,2,1,0:T(8,128)(2,1)S(1)} %pad_maximum_fusion), channel_id=1, source_target_pairs={{0,64},{8,72},{16,80},{24,88},{32,96},{40,104},{48,112},{56,120},{... | collective-permute-start | bytes 1572872 | tf_op jit(solution)/shard_map/ppermute | solution.py:36
  79.2 26.7 %collective-permute-start.4 = (bf16[16,2,128,128]{3,2,1,0:T(8,128)(2,1)}, bf16[16,2,128,128]{3,2,1,0:T(8,128)(2,1)S(1)}, u32[]{:S(2)}, u32[]{:S(2)}) collective-permute-start(bf16[16,2,128,128]{3,2,1,0:T(8,128)(2,1)} %constant_dynamic-update-slice_fusion), channel_id=1, source_target_pairs={{0,128},{8,136},{16,144},{24,152},{32,160},{40,168},{48,176},{56,1... | collective-permute-start | bytes 3145736 | tf_op jit(solution)/shard_map/ppermute | solution.py:36
  85.2 65.7 %copy-start.2 = (bf16[2048,128]{1,0:T(8,128)(2,1)S(1)}, bf16[2048,128]{1,0:T(8,128)(2,1)}, u32[]{:S(2)}) copy-start(bf16[2048,128]{1,0:T(8,128)(2,1)} %param.19) | copy-start | bytes 1572868
  85.5 66.8 %copy-start.5 = (f32[2]{0:T(128)S(1)}, f32[2]{0:T(128)}, u32[]{:S(2)}) copy-start(f32[2]{0:T(128)} %param.26) | copy-start | bytes 28
  110.4 81.1 %collective-permute-start.5 = (bf16[32,2,128,128]{3,2,1,0:T(8,128)(2,1)}, bf16[32,2,128,128]{3,2,1,0:T(8,128)(2,1)}, u32[]{:S(2)}, u32[]{:S(2)}) collective-permute-start(bf16[32,2,128,128]{3,2,1,0:T(8,128)(2,1)} %constant_dynamic-update-slice_fusion.5), channel_id=1, source_target_pairs={{0,256},{8,264},{16,272},{24,280},{32,288},{40,296},{48,304},{56,3... | collective-permute-start | bytes 6291464 | tf_op jit(solution)/shard_map/ppermute | solution.py:36
  149.6 2.3 collective-permute-start.6
  205.9 7.3 %copy-start.8 = (f32[2]{0:T(128)S(1)}, f32[2]{0:T(128)}, u32[]{:S(2)}) copy-start(f32[2]{0:T(128)} %param.25) | copy-start | bytes 28
  213.3 81.8 %copy-start.6 = (f32[128]{0:T(128)S(1)}, f32[128]{0:T(128)}, u32[]{:S(2)}) copy-start(f32[128]{0:T(128)} %param.28) | copy-start | bytes 1540
  213.3 81.8 %copy-start.7 = (f32[128]{0:T(128)S(1)}, f32[128]{0:T(128)}, u32[]{:S(2)}) copy-start(f32[128]{0:T(128)} %param.27) | copy-start | bytes 1540
  284.7 167.5 %copy-start.4 = (f32[2048]{0:T(1024)S(1)}, f32[2048]{0:T(1024)}, u32[]{:S(2)}) copy-start(f32[2048]{0:T(1024)} %param.31) | copy-start | bytes 24580
Sparse Core Ops, SparseCore 0:
  297.8 153.3 reduce-scatter.1
where the time goes:
time: 462 us; the launch traced here: 461 us
  waiting for transfers between devices  235 us (51%)
  starting transfers between devices  68.4 us (15%)
  other arithmetic  52.3 us (11%)
  local copies, waits for them, and re-layouts  44.2 us (10%)
  blocking collectives  28.8 us (6%)
  matrix products  17.5 us (4%)
  between operations  13.7 us (3%)
    reduce_scatter x1, waiting for transfers between devices, shards(): lax.psum_scatter((total + jnp.dot(window_normed, w_out_window, preferred_...  154 us
    ppermute x7, waiting for transfers between devices, passed_along(): lax.ppermute(value, axis, [(source, source + steps) for source in range(i...  81.4 us
    ppermute x7, starting transfers between devices, passed_along(): lax.ppermute(value, axis, [(source, source + steps) for source in range(i...  68.4 us
    all_to_all x2, blocking collectives, from_everyone(): lax.all_to_all(jnp.broadcast_to(array[None], (size, *array.shape)), axis,...  28.8 us
    another operation x16, other arithmetic  20.6 us
    unnamed x35, local copies, waits for them, and re-layouts  14.9 us
    convert_element_type x8, other arithmetic, stick_block(): stick_weights = stick_weights.astype(jnp.bfloat16)  12 us
  transfers between devices with their start and end apart: 8, of which 8 were waited for; matrix products, arithmetic and copies ran while one was open for 1% of the time, Pallas kernels for 0%

commit v1 on v0

v1 whole, which is shorter than its diff:
```python
import jax
import jax.numpy as jnp
from jax import lax
from jax.experimental import pallas as pl
from jax.experimental.pallas import tpu as pltpu
from jax.sharding import Mesh, PartitionSpec as P

HEAD_DIM = 64
WINDOW = 128
TILE = 128
SB_WIDTH = 1024
SW_WIDTH = 1024
ROWS = 8
LOG2E = 1.4426950408889634
SCALE = HEAD_DIM ** (-0.5)

epsilon = 1e-06
f32 = jnp.float32
bf16 = jnp.bfloat16

VM = pl.BlockSpec(memory_space=pltpu.VMEM)
SM = pl.BlockSpec(memory_space=pltpu.SMEM)


def call(kernel, out_shape, in_specs, scratch=(), name=None):
    many = isinstance(out_shape, (tuple, list))
    return pl.pallas_call(
        kernel,
        out_shape=out_shape,
        in_specs=in_specs,
        out_specs=[VM] * len(out_shape) if many else VM,
        scratch_shapes=list(scratch),
        name=name,
    )


def dot(a, b, ca=1, cb=0):
    return lax.dot_general(a, b, (((ca,), (cb,)), ((), ())), preferred_element_type=f32)


def split(value):
    high = value.astype(bf16)
    return high, (value - high.astype(f32)).astype(bf16)


def project_kernel(tok, gain, wqs, wks, wvs, wqw, wkw, wvw, q_out, kv_out, qw_out, kvw_out):
    parts = tok.shape[0]
    wide = [tok[i].astype(f32) for i in range(parts)]
    total = sum(jnp.sum(w * w, axis=1, keepdims=True) for w in wide)
    width = parts * tok.shape[2]
    scale = lax.rsqrt(total / width + epsilon)
    step = tok.shape[2]
    normed = jnp.concatenate(
        [(w * scale * gain[:, i * step : (i + 1) * step]).astype(bf16) for i, w in enumerate(wide)], axis=1
    )
    query = dot(normed, wqs[...]).astype(bf16)
    key = dot(normed, wks[...]).astype(bf16)
    value = dot(normed, wvs[...]).astype(bf16)
    for i in range(q_out.shape[0]):
        q_out[i] = query
    for i in range(kv_out.shape[0]):
        kv_out[i, 0] = key
        kv_out[i, 1] = value
    qw_out[...] = dot(normed, wqw[...]).astype(bf16)
    kvw_out[:, :HEAD_DIM] = dot(normed, wkw[...]).astype(bf16)
    kvw_out[:, HEAD_DIM:] = dot(normed, wvw[...]).astype(bf16)


def stick_kernel(place, bias, q, kv, out, score, weight):
    row = place[0]
    col = place[1]
    blocks = kv.shape[0]
    r_i = lax.broadcasted_iota(jnp.int32, (2 * TILE, 2 * TILE), 0) % TILE
    c_i = lax.broadcasted_iota(jnp.int32, (2 * TILE, 2 * TILE), 1)
    sums = jnp.where((c_i >= TILE) | (r_i >= c_i), 1.0, 0.0).astype(bf16)
    lane = lax.broadcasted_iota(jnp.int32, (TILE, TILE), 1)
    subl = lax.broadcasted_iota(jnp.int32, (TILE, TILE), 0)
    first = lane < HEAD_DIM
    keys = [kv[j, 0] for j in range(blocks)]
    bias2 = [bias[0] * LOG2E, bias[1] * LOG2E]

    def clear(block, _):
        out[block] = jnp.zeros(out.shape[1:], bf16)
        return 0

    lax.fori_loop(0, row, clear, 0)

    def block_step(block, masked):
        query = q[block].astype(f32)
        both = jnp.concatenate([jnp.where(first, query, 0.0), jnp.where(first, 0.0, query)], axis=0).astype(bf16)
        for j in range(blocks):
            score[:, j * TILE : (j + 1) * TILE] = dot(both, keys[j], 1, 1)
        carry = [jnp.zeros((TILE, TILE), f32)] * 2
        for j in reversed(range(blocks)):
            if masked:
                seen = (j * TILE + lane) < (col * TILE + subl)
            for h in range(2):
                rows = slice(h * TILE, (h + 1) * TILE)
                cols = slice(j * TILE, (j + 1) * TILE)
                s = score[rows, cols] * (SCALE * LOG2E) + bias2[h]
                soft = jnp.maximum(s, 0.0) + lax.log2(1.0 + jnp.exp2(-jnp.abs(s)))
                if masked:
                    soft = jnp.where(seen, soft, 0.0)
                high, low = split(soft)
                both_sums = dot(jnp.concatenate([high, low], axis=1), sums)
                w = jnp.exp2(s - both_sums[:, :TILE] - carry[h])
                if masked:
                    w = jnp.where(seen, w, 0.0)
                weight[rows, cols] = w.astype(bf16)
                carry[h] = carry[h] + both_sums[:, TILE:]
        acc = jnp.zeros((2 * TILE, TILE), f32)
        for j in range(0, blocks, 2):
            pair = jnp.concatenate([kv[j, 1], kv[j + 1, 1]], axis=0)
            acc = acc + dot(weight[:, j * TILE : (j + 2) * TILE], pair)
        out[block, :TILE] = jnp.where(first, acc[:TILE], acc[TILE:]).astype(bf16)
        high0, low0 = split(carry[0])
        high1, low1 = split(carry[1])
        tall = jnp.where(
            lane == 0,
            high0.astype(f32),
            jnp.where(lane == 1, low0.astype(f32), jnp.where(lane == 2, high1.astype(f32), low1.astype(f32))),
        )
        out[block, TILE:] = jnp.transpose(tall)[:16].astype(bf16)

    block_step(row, True)

    def later(block, _):
        block_step(block, False)
        return 0

    lax.fori_loop(row + 1, out.shape[0], later, 0)


def window_kernel(has_prev, sinks, qw, prev, own, w_out, gain, prod_out, ssq_out):
    lane = lax.broadcasted_iota(jnp.int32, (TILE, TILE), 1)
    first = lane < HEAD_DIM
    query = qw[...].astype(f32)
    both = jnp.concatenate(
        [jnp.where(first, query, 0.0), jnp.where(first, pltpu.roll(query, HEAD_DIM, 1), 0.0)], axis=0
    ).astype(bf16)
    pair = jnp.concatenate([prev[...], own[...]], axis=0)
    logits = dot(both, pair, 1, 1) * SCALE
    r_i = lax.broadcasted_iota(jnp.int32, (2 * TILE, 2 * TILE), 0)
    c_i = lax.broadcasted_iota(jnp.int32, (2 * TILE, 2 * TILE), 1)
    distance = r_i % TILE + WINDOW - c_i
    usable = (distance >= 0) & (distance < WINDOW) & ((c_i >= TILE) | (has_prev[0] > 0))
    logits = jnp.where(usable, logits, -jnp.inf)
    sink = jnp.where(r_i[:, :1] < TILE, sinks[0], sinks[1])
    top = jnp.maximum(jnp.max(logits, axis=1, keepdims=True), sink)
    powers = jnp.exp(logits - top)
    total = jnp.sum(powers, axis=1, keepdims=True) + jnp.exp(sink - top)
    weights = (powers / total).astype(bf16)
    mixed = dot(weights, pair)
    result = jnp.where(first, pltpu.roll(mixed[:TILE], HEAD_DIM, 1), mixed[TILE:]).astype(bf16).astype(f32)
    ssq_out[...] = jnp.broadcast_to(jnp.sum(result * result, axis=1, keepdims=True), (TILE, TILE))
    scaled = (result * gain[...]).astype(bf16)
    prod_out[...] = dot(scaled, w_out[...]).astype(bf16)


def combine_kernel(parts, gain, w_out, prod_w, ssq_w, out):
    count = parts.shape[0]
    width = w_out.shape[1]
    lane = lax.broadcasted_iota(jnp.int32, (TILE, TILE), 1)
    first = lane < HEAD_DIM
    rows = [parts[z, TILE:].astype(f32) for z in range(count)]
    after = [jnp.zeros((1, TILE), f32)] * 2
    factors = [[None] * count, [None] * count]
    for z in reversed(range(count)):
        for h in range(2):
            factors[h][z] = jnp.exp2(-after[h])
            after[h] = after[h] + rows[z][2 * h : 2 * h + 1] + rows[z][2 * h + 1 : 2 * h + 2]
    tall = jnp.transpose(
        jnp.concatenate(factors[0] + factors[1] + [jnp.zeros((TILE - 2 * count, TILE), f32)], axis=0)
    )
    result = jnp.zeros((TILE, TILE), f32)
    for z in range(count):
        factor = jnp.where(first, tall[:, z : z + 1], tall[:, count + z : count + z + 1])
        result = result + factor * parts[z, :TILE].astype(f32)
    result = result.astype(bf16).astype(f32)
    ssq = jnp.sum(result * result, axis=1, keepdims=True)
    scaled = (result * gain[...]).astype(bf16)
    out[:, :width] = dot(scaled, w_out[...]).astype(bf16)
    out[:, width : 2 * width] = prod_w[...]
    high_s, low_s = split(jnp.broadcast_to(ssq, (TILE, TILE)))
    high_w, low_w = split(ssq_w[...])
    out[:, 2 * width :] = jnp.where(
        lane == 0,
        high_s.astype(f32),
        jnp.where(lane == 1, low_s.astype(f32), jnp.where(lane == 2, high_w.astype(f32), low_w.astype(f32))),
    ).astype(bf16)


def final_kernel(parts, gain, out):
    width = out.shape[1]
    count = parts.shape[0]
    squares = sum(parts[i, :, 2 * width :].astype(f32) for i in range(count))
    stick = lax.rsqrt((squares[:, 0:1] + squares[:, 1:2]) / SB_WIDTH + epsilon)
    window = lax.rsqrt((squares[:, 2:3] + squares[:, 3:4]) / SW_WIDTH + epsilon)
    sum_s = sum(parts[i, :, :width].astype(f32) for i in range(count))
    sum_w = sum(parts[i, :, width : 2 * width].astype(f32) for i in range(count))
    combined = (sum_s * stick + sum_w * window).astype(bf16).astype(f32)
    mean = jnp.mean(combined * combined, axis=1, keepdims=True)
    out[...] = (combined * lax.rsqrt(mean + epsilon) * gain[...]).astype(bf16)


def shards(
    tokens,
    pre_gain,
    w_query_stick,
    w_key_stick,
    w_value_stick,
    w_query_window,
    w_key_window,
    w_value_window,
    stick_bias,
    sinks,
    stick_gain,
    window_gain,
    w_out_stick,
    w_out_window,
    post_gain,
):
    tok_rows, feats = tokens.shape
    nz, ny, ntp = lax.axis_size("z"), lax.axis_size("y"), lax.axis_size("tp")
    z, y = lax.axis_index("z"), lax.axis_index("y")
    width = ntp * feats

    def swap(value, axis):
        return lax.all_to_all(value, axis, 0, 0, tiled=True)

    gathered = lax.all_gather(tokens, "tp", axis=0, tiled=True).reshape(ntp, tok_rows, feats)
    pair_width = w_key_stick.shape[1]
    q_all, kv_all, q_win, kv_win = call(
        project_kernel,
        (
            jax.ShapeDtypeStruct((nz, tok_rows, pair_width), bf16),
            jax.ShapeDtypeStruct((ny, 2, tok_rows, pair_width), bf16),
            jax.ShapeDtypeStruct((tok_rows, pair_width), bf16),
            jax.ShapeDtypeStruct((tok_rows, pair_width), bf16),
        ),
        [VM] * 8,
        name="project",
    )(
        gathered,
        pre_gain.reshape(1, width),
        w_query_stick,
        w_key_stick,
        w_value_stick,
        w_query_window,
        w_key_window,
        w_value_window,
    )
    count = nz * ny
    previous = lax.ppermute(kv_win, ("z", "y"), [(i, i + 1) for i in range(count - 1)])
    kv_row = swap(kv_all, "y")
    q_col = swap(q_all, "z")
    index = z * ny + y
    prod_w, ssq_w = call(
        window_kernel,
        (jax.ShapeDtypeStruct((tok_rows, width), bf16), jax.ShapeDtypeStruct((tok_rows, TILE), f32)),
        [SM, SM] + [VM] * 5,
        name="window",
    )(index.reshape(1), sinks, q_win, previous, kv_win, w_out_window, window_gain.reshape(1, -1))
    partial = call(
        stick_kernel,
        jax.ShapeDtypeStruct((nz, TILE + 16, TILE), bf16),
        [SM, SM, VM, VM],
        scratch=[
            pltpu.VMEM((2 * TILE, ny * TILE), f32),
            pltpu.VMEM((2 * TILE, ny * TILE), bf16),
        ],
        name="stick",
    )(jnp.stack([z, y]), stick_bias, q_col, kv_row)
    returned = swap(partial, "z")
    sending = call(
        combine_kernel,
        jax.ShapeDtypeStruct((tok_rows, 2 * width + TILE), bf16),
        [VM] * 5,
        name="combine",
    )(returned, stick_gain.reshape(1, -1), w_out_stick, prod_w, ssq_w)
    arrived = swap(sending.reshape(ntp, tok_rows // ntp, 2 * width + TILE), "tp")
    return call(
        final_kernel, jax.ShapeDtypeStruct((tok_rows // ntp, width), bf16), [VM, VM], name="final"
    )(arrived, post_gain.reshape(1, width))


def solution(mesh):
    cube = Mesh(mesh.devices.reshape(-1, ROWS, mesh.devices.shape[-1]), ("z", "y", "tp"))
    seq = ("z", "y")
    in_specs = (
        P(seq, "tp"),
        P(),
        P(None, "tp"),
        P(None, "tp"),
        P(None, "tp"),
        P(None, "tp"),
        P(None, "tp"),
        P(None, "tp"),
        P("tp"),
        P("tp"),
        P("tp"),
        P("tp"),
        P("tp", None),
        P("tp", None),
        P(),
    )
    out_specs = P(("z", "y", "tp"), None)
    return jax.shard_map(shards, mesh=cube, in_specs=in_specs, out_specs=out_specs, check_vma=False)
```

time: 462 us -> 126 us (0.27)
  waiting for transfers between devices: 235 us -> 26.3 us
  starting transfers between devices: 68.4 us -> 11.5 us
  other arithmetic: 52.3 us -> 0.67 us
  local copies, waits for them, and re-layouts: 44.2 us -> 5.1 us
  blocking collectives: 28.8 us -> 59.1 us
  Pallas kernels: 0 us -> 23.1 us
  matrix products: 17.5 us -> 0 us
  between operations: 13.7 us -> 0.05 us
    reduce_scatter x1 -> x0, waiting for transfers between devices: 154 us -> none  [shards(): lax.psum_scatter((total + jnp.dot(window_normed, w_out_window, preferred_...]
    ppermute x7 -> x1, waiting for transfers between devices: 81.4 us -> 1 us  [shards(): lax.ppermute(kv_win, ('z', 'y'), [(i, i + 1) for i in range(count - 1)])]
    ppermute x7 -> x1, starting transfers between devices: 68.4 us -> 1.29 us  [shards(): lax.ppermute(kv_win, ('z', 'y'), [(i, i + 1) for i in range(count - 1)])]
    all_to_all x0 -> x2, waiting for transfers between devices: none -> 25.3 us  [swap(): return lax.all_to_all(value, axis, 0, 0, tiled=True)]
    pallas_call x0 -> x5, Pallas kernels: none -> 23.1 us  [the longest x1 11.3 us: shards(): call(stick_kernel, jax.ShapeDtypeStruct((nz, TILE + 16, TILE), bf16), [SM...]
    all_gather x0 -> x1, blocking collectives: none -> 21.2 us  [shards(): lax.all_gather(tokens, 'tp', axis=0, tiled=True)]
    another operation x25 -> x1, other arithmetic: 21.1 us -> 0.67 us  [shards(): jnp.stack([z, y])]
    dot_general x26 -> x0, matrix products: 17.5 us -> none  [the longest x8 7.85 us: stick_block(): jnp.einsum('thd,shd->hts', queries, key_rows, preferred_element_type=jnp....]
  transfers between devices with their start and end apart: 8 -> 3, of which waited for: 8 -> 3; matrix products, arithmetic and copies ran while one was open for 1% -> 1% of each run, Pallas kernels for 0% -> 2%
where the time goes in v1:
time: 126 us
  blocking collectives  59.1 us (47%)
  waiting for transfers between devices  26.3 us (21%)
  Pallas kernels  23.1 us (18%)
  starting transfers between devices  11.5 us (9%)
  local copies, waits for them, and re-layouts  5.1 us (4%)
    all_to_all x2, blocking collectives, swap(): return lax.all_to_all(value, axis, 0, 0, tiled=True)  37.9 us
    all_to_all x2, waiting for transfers between devices, swap(): return lax.all_to_all(value, axis, 0, 0, tiled=True)  25.3 us
    all_gather x1, blocking collectives, shards(): lax.all_gather(tokens, 'tp', axis=0, tiled=True)  21.2 us
    pallas_call x1, Pallas kernels, shards(): call(stick_kernel, jax.ShapeDtypeStruct((nz, TILE + 16, TILE), bf16), [SM...  11.3 us
    all_to_all x2, starting transfers between devices, swap(): return lax.all_to_all(value, axis, 0, 0, tiled=True)  10.2 us
    unnamed x12, local copies, waits for them, and re-layouts  5.1 us
    pallas_call x1, Pallas kernels, shards(): call(project_kernel, (jax.ShapeDtypeStruct((nz, tok_rows, pair_width), bf...  3.84 us
    pallas_call x1, Pallas kernels, shards(): call(combine_kernel, jax.ShapeDtypeStruct((tok_rows, 2 * width + TILE), b...  3.1 us
  transfers between devices with their start and end apart: 3, of which 3 were waited for; matrix products, arithmetic and copies ran while one was open for 1% of the time, Pallas kernels for 2%

profile of v1, /device:TPU:1, one launch (start us, length us, event | category | flops | bytes accessed | tf_op | source)
XLA Modules:
  0.0 125.8 jit_solution(6839997746399211543)
XLA Ops:
  0.0 0.0 copy-start.2
  0.0 21.2 %all_gather.3 = bf16[1024,256]{1,0:T(8,128)(2,1)} all-gather(bf16[128,256]{1,0:T(8,128)(2,1)} %param.15), channel_id=1, replica_groups=mesh['z'=8,'y'=8,'tp'=8] {'tp'}, dimensions={0}, use_global_device_ids=true | all-gather | bytes 589824 | tf_op jit(solution)/shard_map/all_gather | solution.py:231
  21.2 2.0 %copy.16.wkw = bf16[2048,64]{1,0:T(8,128)(2,1)} copy(bf16[2048,64]{0,1:T(8,128)(2,1)} %param.21) | data formatting | bytes 524288 | tf_op args[6]
  23.2 0.0 copy-done.2
  23.2 1.0 copy.17.wvw
  24.2 3.8 %project.1 = (bf16[8,128,128]{2,1,0:T(8,128)(2,1)}, bf16[8,2,128,128]{3,2,1,0:T(8,128)(2,1)}, bf16[128,128]{1,0:T(8,128)(2,1)}, bf16[128,128]{1,0:T(8,128)(2,1)}) custom-call(bf16[8,128,256]{2,1,0:T(8,128)(2,1)} %bitcast.10, f32[1,2048]{1,0:T(1,128)} %bitcast.11, bf16[2048,128]{1,0:T(8,128)(2,1)} %wqs.1, bf16[2048,128]{1,0:T(8,128)(2,1)} %wks.1, ...), custom_call_target="tpu_custom_call" | custom-call | tf_op jit(solution)/shard_map/project/pallas_call | solution.py:233
  28.0 17.4 %all_to_all.20.q = bf16[8,128,128]{2,1,0:T(8,128)(2,1)} all-to-all(bf16[8,128,128]{2,1,0:T(8,128)(2,1)} %get-tuple-element.11), channel_id=1, replica_groups=mesh['z'=8,'y'=8,'tp'=8] {'z'}, dimensions={0} | all-to-all | bytes 524288 | tf_op jit(solution)/shard_map/all_to_all | solution.py:229
  45.4 6.8 %all-to-all-start.1 = ((bf16[8,2,128,128]{3,2,1,0:T(8,128)(2,1)}), bf16[8,2,128,128]{3,2,1,0:T(8,128)(2,1)S(1)}, u32[]{:S(2)}, u32[]{:S(2)}) async-start(bf16[8,2,128,128]{3,2,1,0:T(8,128)(2,1)} %get-tuple-element.12), calls=%async_computation.1 | async-start | bytes 1048576 | tf_op jit(solution)/shard_map/all_to_all | solution.py:229
  52.2 0.0 copy-start.3
  52.2 0.7 pad_add_fusion.place
  52.9 17.3 %all-to-all-done.1.kv = bf16[8,2,128,128]{3,2,1,0:T(8,128)(2,1)S(1)} async-done(((bf16[8,2,128,128]{3,2,1,0:T(8,128)(2,1)}), bf16[8,2,128,128]{3,2,1,0:T(8,128)(2,1)S(1)}, u32[]{:S(2)}, u32[]{:S(2)}) %all-to-all-start.1) | async-done | bytes 524320 | tf_op jit(solution)/shard_map/all_to_all | solution.py:229
  70.2 0.0 copy-start
  70.2 0.8 copy-done
  71.0 11.3 %stick.1 = bf16[8,144,128]{2,1,0:T(8,128)(2,1)} custom-call(s32[2]{0:T(128)} %pad_add_fusion.place, f32[2]{0:T(128)} %bias.1, bf16[8,128,128]{2,1,0:T(8,128)(2,1)} %all_to_all.20.q, bf16[8,2,128,128]{3,2,1,0:T(8,128)(2,1)} %copy-done), custom_call_target="tpu_custom_call" | custom-call | tf_op jit(solution)/shard_map/stick/pallas_call | solution.py:264
  82.2 3.4 %all-to-all-start.2 = ((bf16[8,144,128]{2,1,0:T(8,128)(2,1)}), bf16[8,144,128]{2,1,0:T(8,128)(2,1)S(1)}, u32[]{:S(2)}, u32[]{:S(2)}) async-start(bf16[8,144,128]{2,1,0:T(8,128)(2,1)} %stick.1), calls=%async_computation.2 | async-start | bytes 589824 | tf_op jit(solution)/shard_map/all_to_all | solution.py:229
  85.7 0.0 copy-done.3
  85.7 1.3 %collective-permute-start = (bf16[128,128]{1,0:T(8,128)(2,1)S(1)}, bf16[128,128]{1,0:T(8,128)(2,1)S(1)}, u32[]{:S(2)}, u32[]{:S(2)}) collective-permute-start(bf16[128,128]{1,0:T(8,128)(2,1)S(1)} %copy-done.3), channel_id=1, source_target_pairs={{0,8},{8,16},{16,24},{24,32},{32,40},{40,48},{48,56},{56,64},{64,7... | collective-permute-start | bytes 98312 | tf_op jit(solution)/shard_map/ppermute | solution.py:254
  87.0 1.0 collective-permute-done.prev
  88.0 0.0 copy-start.4
  88.0 0.6 copy-done.4
  88.6 2.7 %window.1 = (bf16[128,2048]{1,0:T(8,128)(2,1)}, f32[128,128]{1,0:T(8,128)}) custom-call(s32[1]{0:T(128)} %bitcast.5.has_prev, f32[2]{0:T(128)} %sinks.1, bf16[128,128]{1,0:T(8,128)(2,1)} %get-tuple-element.13.qw, bf16[128,128]{1,0:T(8,128)(2,1)} %copy-done.4, bf16[128,128]{1,0:T(8,128)(2,1)} %get-tuple-element.14.own, bf16[128,2048]{1,0:T(8,128)(2,1)} %w_out.2, ...), custom_call_target="tpu_custom_call" | custom-call | tf_op jit(solution)/shard_map/window/pallas_call | solution.py:258
  91.3 8.0 %all-to-all-done.2.parts = bf16[8,144,128]{2,1,0:T(8,128)(2,1)S(1)} async-done(((bf16[8,144,128]{2,1,0:T(8,128)(2,1)}), bf16[8,144,128]{2,1,0:T(8,128)(2,1)S(1)}, u32[]{:S(2)}, u32[]{:S(2)}) %all-to-all-start.2) | async-done | bytes 294944 | tf_op jit(solution)/shard_map/all_to_all | solution.py:229
  99.3 0.0 copy-start.1
  99.3 0.7 copy-done.1
  100.0 3.1 %combine.1 = bf16[128,4224]{1,0:T(8,128)(2,1)} custom-call(bf16[8,144,128]{2,1,0:T(8,128)(2,1)} %copy-done.1, f32[1,128]{1,0:T(1,128)} %bitcast.14, bf16[128,2048]{1,0:T(8,128)(2,1)} %w_out.3, bf16[128,2048]{1,0:T(8,128)(2,1)} %get-tuple-element.15.prod_w, f32[128,128]{1,0:T(8,128)} %get-tuple-element.16.ssq_w), custom_call_target="tpu_custom_call" | custom-call | tf_op jit(solution)/shard_map/combine/pallas_call | solution.py:275
  103.1 20.5 %all_to_all.21.parts = bf16[8,16,4224]{2,1,0:T(8,128)(2,1)} all-to-all(bf16[8,16,4224]{2,1,0:T(8,128)(2,1)} %bitcast.9), channel_id=1, replica_groups=mesh['z'=8,'y'=8,'tp'=8] {'tp'}, dimensions={0} | all-to-all | bytes 2162688 | tf_op jit(solution)/shard_map/all_to_all | solution.py:229
  123.6 2.2 %final.1 = bf16[16,2048]{1,0:T(8,128)(2,1)} custom-call(bf16[8,16,4224]{2,1,0:T(8,128)(2,1)} %all_to_all.21.parts, f32[1,2048]{1,0:T(1,128)} %bitcast.12), custom_call_target="tpu_custom_call" | custom-call | tf_op jit(solution)/shard_map/final/pallas_call | solution.py:282
Async XLA Ops:
  0.0 23.2 %copy-start.2 = (bf16[2048,64]{0,1:T(8,128)(2,1)S(1)}, bf16[2048,64]{0,1:T(8,128)(2,1)}, u32[]{:S(2)}) copy-start(bf16[2048,64]{0,1:T(8,128)(2,1)} %param.22) | copy-start | bytes 786436
  45.4 24.8 %all-to-all-start.1 = ((bf16[8,2,128,128]{3,2,1,0:T(8,128)(2,1)}), bf16[8,2,128,128]{3,2,1,0:T(8,128)(2,1)S(1)}, u32[]{:S(2)}, u32[]{:S(2)}) async-start(bf16[8,2,128,128]{3,2,1,0:T(8,128)(2,1)} %get-tuple-element.12), calls=%async_computation.1 | async-start | bytes 1048576 | tf_op jit(solution)/shard_map/all_to_all | solution.py:229
  52.2 33.5 %copy-start.3 = (bf16[128,128]{1,0:T(8,128)(2,1)S(1)}, bf16[128,128]{1,0:T(8,128)(2,1)}, u32[]{:S(2)}) copy-start(bf16[128,128]{1,0:T(8,128)(2,1)} %get-tuple-element.14.own) | copy-start | bytes 98308
  70.2 0.8 copy-start
  82.2 17.0 %all-to-all-start.2 = ((bf16[8,144,128]{2,1,0:T(8,128)(2,1)}), bf16[8,144,128]{2,1,0:T(8,128)(2,1)S(1)}, u32[]{:S(2)}, u32[]{:S(2)}) async-start(bf16[8,144,128]{2,1,0:T(8,128)(2,1)} %stick.1), calls=%async_computation.2 | async-start | bytes 589824 | tf_op jit(solution)/shard_map/all_to_all | solution.py:229
  85.7 2.3 %collective-permute-start = (bf16[128,128]{1,0:T(8,128)(2,1)S(1)}, bf16[128,128]{1,0:T(8,128)(2,1)S(1)}, u32[]{:S(2)}, u32[]{:S(2)}) collective-permute-start(bf16[128,128]{1,0:T(8,128)(2,1)S(1)} %copy-done.3), channel_id=1, source_target_pairs={{0,8},{8,16},{16,24},{24,32},{32,40},{40,48},{48,56},{56,64},{64,7... | collective-permute-start | bytes 98312 | tf_op jit(solution)/shard_map/ppermute | solution.py:254
  88.0 0.6 copy-start.4
  99.3 0.7 copy-start.1

commit v2 on v1

v2 whole, which is shorter than its diff:
```python
import jax
import jax.numpy as jnp
from jax import lax
from jax.experimental import pallas as pl
from jax.experimental.pallas import tpu as pltpu
from jax.sharding import Mesh, PartitionSpec as P


HEAD_DIM = 64
WINDOW = 128
TILE = 128
SB_WIDTH = 1024
SW_WIDTH = 1024
ROWS = 8
TAIL = 8
PIECES = 4
LOG2E = 1.4426950408889634
SCALE = HEAD_DIM ** (-0.5)

epsilon = 1e-06
f32 = jnp.float32
bf16 = jnp.bfloat16

VM = pl.BlockSpec(memory_space=pltpu.VMEM)
SM = pl.BlockSpec(memory_space=pltpu.SMEM)
HB = pl.BlockSpec(memory_space=pltpu.HBM)


def call(kernel, out_shape, in_specs, scratch=(), keep=True):
    many = isinstance(out_shape, (tuple, list))
    shapes = out_shape if many else [out_shape]
    if keep:
        shapes = [pltpu.VMEM(s.shape, s.dtype) for s in shapes]
    run = pl.pallas_call(
        kernel,
        out_shape=shapes if many else shapes[0],
        in_specs=in_specs,
        out_specs=[VM] * len(shapes) if many else VM,
        scratch_shapes=list(scratch),
        compiler_params=pltpu.CompilerParams(vmem_limit_bytes=16 * 2**20),
    )

    def begun(*args):
        spaces = {id(VM): pltpu.VMEM, id(HB): pltpu.HBM}
        return run(
            *[
                pltpu.with_memory_space_constraint(a, spaces[id(spec)]) if id(spec) in spaces else a
                for a, spec in zip(args, in_specs)
            ]
        )

    return begun


def dot(a, b, ca=1, cb=0):
    return lax.dot_general(a, b, (((ca,), (cb,)), ((), ())), preferred_element_type=f32)


def split(value):
    high = value.astype(bf16)
    return high, (value - high.astype(f32)).astype(bf16)


def fetched(sources, holders, sems):
    copies = []
    for source, holder in zip(sources, holders):
        step = source.shape[0] // PIECES if source.shape[0] % (8 * PIECES) == 0 else source.shape[0]
        copies.append([])
        for at in range(0, source.shape[0], step):
            piece = pl.ds(at, step)
            number = sum(map(len, copies))
            copies[-1].append(pltpu.make_async_copy(source.at[piece], holder.at[piece], sems.at[number]))
    for copy in sum(copies, []):
        copy.start()

    def ready(at):
        for copy in copies[at]:
            copy.wait()
        return holders[at][...]

    return ready


def keys_kernel(tok, gain, wk, wv, kv_out, normed_out, *held):
    ready = fetched((wk, wv, gain), held[:3], held[3])
    parts = tok.shape[0]
    wide = [tok[i].astype(f32) for i in range(parts)]
    total = sum(jnp.sum(w * w, axis=1, keepdims=True) for w in wide)
    scale = lax.rsqrt(total / (parts * tok.shape[2]) + epsilon)
    step = tok.shape[2]
    gains = ready(2)
    for i, w in enumerate(wide):
        normed_out[:, i * step : (i + 1) * step] = (w * scale * gains[:, i * step : (i + 1) * step]).astype(bf16)
    normed = normed_out[...]
    key = dot(normed, ready(0))
    value = dot(normed, ready(1))
    first = lax.broadcasted_iota(jnp.int32, (TILE, TILE), 1) < HEAD_DIM
    heads = [
        jnp.where(first, key, pltpu.roll(value, HEAD_DIM, 1)).astype(bf16),
        jnp.where(first, pltpu.roll(key, HEAD_DIM, 1), value).astype(bf16),
    ]
    for i in range(kv_out.shape[0]):
        kv_out[i] = heads[i % 2]


def rest_kernel(normed_in, wq, wqw, wkw, wvw, q_out, qw_out, kvw_out, *held):
    ready = fetched((wkw, wvw, wq, wqw), held[:4], held[4])
    normed = normed_in[...]
    kvw_out[:, :HEAD_DIM] = dot(normed, ready(0), 1, 1).astype(bf16)
    kvw_out[:, HEAD_DIM:] = dot(normed, ready(1), 1, 1).astype(bf16)
    query = dot(normed, ready(2)).astype(bf16)
    turned = jnp.transpose(query.astype(f32)).astype(bf16)
    for i in range(q_out.shape[0]):
        q_out[i, 0] = turned[:HEAD_DIM]
        q_out[i, 1] = turned[HEAD_DIM:]
    qw_out[...] = dot(normed, ready(3)).astype(bf16)


def stick_kernel(bias, q, kv, out, weight, keys, values):
    row = lax.axis_index("z")
    duo = lax.axis_index("yy")
    shift = jnp.where(lax.axis_index("hy") == 0, bias[0], bias[1]) * LOG2E
    blocks = kv.shape[0]
    pair = 2 * TILE
    r_i = lax.broadcasted_iota(jnp.int32, (pair, pair), 0)
    c_i = lax.broadcasted_iota(jnp.int32, (pair, pair), 1)
    after = jnp.where(c_i > r_i, 1.0, 0.0).astype(bf16)
    for j in range(blocks):
        cols = slice(j * TILE, (j + 1) * TILE)
        keys[cols] = kv[j, :, :HEAD_DIM]
        values[:, cols] = jnp.transpose(kv[j].astype(f32))[HEAD_DIM:].astype(bf16)

    def clear(block, _):
        out[2 * block] = jnp.zeros(out.shape[1:], bf16)
        out[2 * block + 1] = jnp.zeros(out.shape[1:], bf16)
        return 0

    lax.fori_loop(0, row, clear, 0)

    def block_step(block, masked):
        query = jnp.concatenate([q[2 * block], q[2 * block + 1]], axis=1)
        carry = [jnp.zeros((1, pair), f32)]

        def open_tile(j):
            s = dot(keys[j * TILE : (j + 2) * TILE], query) * (SCALE * LOG2E) + shift
            soft = jnp.maximum(s, lax.log2(1.0 + jnp.exp2(jnp.minimum(s, 126.0))))
            rest = s - soft
            if masked:
                seen = (j * TILE + r_i) < (duo * pair + c_i)
                soft = jnp.where(seen, soft, 0.0)
                rest = jnp.where(seen, rest, -jnp.inf)
            return rest, soft[:1], dot(after, soft.astype(bf16))

        def close_tile(j, rest, own, sums):
            w = jnp.exp2(rest - (sums + carry[0]))
            weight[j * TILE : (j + 2) * TILE] = w.astype(bf16)
            carry[0] = carry[0] + (sums[:1] + own)

        units = list(reversed(range(0, blocks, 2)))
        opened = open_tile(units[0])
        for at, unit in enumerate(units):
            following = open_tile(units[at + 1]) if at + 1 < len(units) else None
            close_tile(unit, *opened)
            opened = following
        acc = dot(values[...], weight[...])
        high, low = split(carry[0])
        tail = lax.broadcasted_iota(jnp.int32, (TAIL, pair), 0)
        tail = jnp.where(tail == 0, high.astype(f32), jnp.where(tail == 1, low.astype(f32), 0.0))
        for i in range(2):
            cols = slice(i * TILE, (i + 1) * TILE)
            out[2 * block + i, :HEAD_DIM] = acc[:, cols].astype(bf16)
            out[2 * block + i, HEAD_DIM:] = tail[:, cols].astype(bf16)

    block_step(row, True)

    def later(block, _):
        block_step(block, False)
        return 0

    lax.fori_loop(row + 1, out.shape[0] // 2, later, 0)


def window_kernel(sinks, qw, prev, own, w_out, gain, prod_out, ssq_out):
    lane = lax.broadcasted_iota(jnp.int32, (TILE, TILE), 1)
    first = lane < HEAD_DIM
    block = lax.axis_index("z") + lax.axis_index("yy") + lax.axis_index("hy")
    query = qw[...].astype(f32)
    both = jnp.concatenate(
        [jnp.where(first, query, 0.0), jnp.where(first, pltpu.roll(query, HEAD_DIM, 1), 0.0)], axis=0
    ).astype(bf16)
    pair = jnp.concatenate([prev[...], own[...]], axis=0)
    logits = dot(both, pair, 1, 1) * SCALE
    r_i = lax.broadcasted_iota(jnp.int32, (2 * TILE, 2 * TILE), 0)
    c_i = lax.broadcasted_iota(jnp.int32, (2 * TILE, 2 * TILE), 1)
    distance = r_i % TILE + WINDOW - c_i
    usable = (distance >= 0) & (distance < WINDOW) & (c_i >= TILE * jnp.where(block > 0, 0, 1))
    logits = jnp.where(usable, logits, -jnp.inf)
    sink = jnp.where(r_i[:, :1] < TILE, sinks[0], sinks[1])
    top = jnp.maximum(jnp.max(logits, axis=1, keepdims=True), sink)
    powers = jnp.exp(logits - top)
    total = jnp.sum(powers, axis=1, keepdims=True) + jnp.exp(sink - top)
    weights = (powers / total).astype(bf16)
    mixed = dot(weights, pair)
    result = jnp.where(first, pltpu.roll(mixed[:TILE], HEAD_DIM, 1), mixed[TILE:]).astype(bf16).astype(f32)
    ssq_out[...] = jnp.broadcast_to(jnp.sum(result * result, axis=1, keepdims=True), (TILE, TILE))
    scaled = (result * gain[...]).astype(bf16)
    prod_out[...] = dot(scaled, w_out[...]).astype(bf16)


def combine_kernel(parts, gain, w_out, prod_w, ssq_w, out):
    count = parts.shape[0] // 2
    width = w_out.shape[1]
    lane = lax.broadcasted_iota(jnp.int32, (TILE, TILE), 1)
    heads = []
    for h in range(2):
        later = jnp.zeros((1, TILE), f32)
        total = jnp.zeros((HEAD_DIM, TILE), f32)
        for z in reversed(range(count)):
            at = 2 * z + h
            total = total + parts[at, :HEAD_DIM].astype(f32) * jnp.exp2(-later)
            tail = parts[at, HEAD_DIM:].astype(f32)
            later = later + tail[0:1] + tail[1:2]
        heads.append(total)
    result = jnp.transpose(jnp.concatenate(heads, axis=0))
    result = result.astype(bf16).astype(f32)
    ssq = jnp.sum(result * result, axis=1, keepdims=True)
    scaled = (result * gain[...]).astype(bf16)
    out[:, :width] = dot(scaled, w_out[...]).astype(bf16)
    out[:, width : 2 * width] = prod_w[...]
    high_s, low_s = split(jnp.broadcast_to(ssq, (TILE, TILE)))
    high_w, low_w = split(ssq_w[...])
    out[:, 2 * width :] = jnp.where(
        lane == 0,
        high_s.astype(f32),
        jnp.where(lane == 1, low_s.astype(f32), jnp.where(lane == 2, high_w.astype(f32), low_w.astype(f32))),
    ).astype(bf16)


def final_kernel(parts, gain, out):
    width = out.shape[1]
    count = parts.shape[0]
    squares = sum(parts[i, :, 2 * width :].astype(f32) for i in range(count))
    stick = lax.rsqrt((squares[:, 0:1] + squares[:, 1:2]) / SB_WIDTH + epsilon)
    window = lax.rsqrt((squares[:, 2:3] + squares[:, 3:4]) / SW_WIDTH + epsilon)
    sum_s = sum(parts[i, :, :width].astype(f32) for i in range(count))
    sum_w = sum(parts[i, :, width : 2 * width].astype(f32) for i in range(count))
    combined = (sum_s * stick + sum_w * window).astype(bf16).astype(f32)
    mean = jnp.mean(combined * combined, axis=1, keepdims=True)
    out[...] = (combined * lax.rsqrt(mean + epsilon) * gain[...]).astype(bf16)


def shards(
    tokens,
    pre_gain,
    w_query_stick,
    w_key_stick,
    w_value_stick,
    w_query_window,
    w_key_window,
    w_value_window,
    stick_bias,
    sinks,
    stick_gain,
    window_gain,
    w_out_stick,
    w_out_window,
    post_gain,
):
    tok_rows, feats = tokens.shape
    nz, ntp = lax.axis_size("z"), lax.axis_size("tp")
    width = ntp * feats

    def swap(value, axis):
        return lax.all_to_all(value, axis, 0, 0, tiled=True)

    gathered = lax.all_gather(tokens, "tp", axis=0, tiled=True).reshape(ntp, tok_rows, feats)
    head_pair = w_key_stick.shape[1]

    def holders(arrays):
        return [pltpu.VMEM(a.shape, a.dtype) for a in arrays] + [pltpu.SemaphoreType.DMA((PIECES * len(arrays),))]

    weights = (w_key_stick, w_value_stick)
    gain = pre_gain.reshape(1, width)
    kv_all, normed = call(
        keys_kernel,
        (
            jax.ShapeDtypeStruct((ROWS, tok_rows, head_pair), bf16),
            jax.ShapeDtypeStruct((tok_rows, width), bf16),
        ),
        [VM, HB, HB, HB],
        scratch=holders(weights + (gain,)),
    )(gathered, gain, *weights)
    kv_row = swap(kv_all, ("yy", "hy"))
    weights = (w_query_stick, w_query_window, w_key_window.T, w_value_window.T)
    q_all, q_win, kv_win = call(
        rest_kernel,
        (
            jax.ShapeDtypeStruct((nz, 2, HEAD_DIM, tok_rows), bf16),
            jax.ShapeDtypeStruct((tok_rows, head_pair), bf16),
            jax.ShapeDtypeStruct((tok_rows, head_pair), bf16),
        ),
        [VM] + [HB] * 4,
        scratch=holders((weights[2], weights[3], weights[0], weights[1])),
    )(normed, *weights)
    count = nz * ROWS
    previous = lax.ppermute(kv_win, ("z", "yy", "hy"), [(i, i + 1) for i in range(count - 1)])
    q_col = swap(q_all.reshape(2 * nz, HEAD_DIM, tok_rows), ("z", "hy"))
    prod_w, ssq_w = call(
        window_kernel,
        (jax.ShapeDtypeStruct((tok_rows, width), bf16), jax.ShapeDtypeStruct((tok_rows, TILE), f32)),
        [SM] + [VM] * 5,
    )(sinks, q_win, previous, kv_win, w_out_window, window_gain.reshape(1, -1))
    partial = call(
        stick_kernel,
        jax.ShapeDtypeStruct((2 * nz, HEAD_DIM + TAIL, TILE), bf16),
        [SM, VM, VM],
        scratch=[
            pltpu.VMEM((ROWS * TILE, 2 * TILE), bf16),
            pltpu.VMEM((ROWS * TILE, HEAD_DIM), bf16),
            pltpu.VMEM((HEAD_DIM, ROWS * TILE), bf16),
        ],
    )(stick_bias, q_col, kv_row)
    returned = swap(partial, ("z", "hy"))
    sending = call(
        combine_kernel, jax.ShapeDtypeStruct((tok_rows, 2 * width + TILE), bf16), [VM] * 5
    )(returned, stick_gain.reshape(1, -1), w_out_stick, prod_w, ssq_w)
    arrived = swap(sending.reshape(ntp, tok_rows // ntp, 2 * width + TILE), "tp")
    return call(
        final_kernel, jax.ShapeDtypeStruct((tok_rows // ntp, width), bf16), [VM, VM], keep=False
    )(arrived, post_gain.reshape(1, width))


def solution(mesh):
    cube = Mesh(mesh.devices.reshape(-1, ROWS // 2, 2, mesh.devices.shape[-1]), ("z", "yy", "hy", "tp"))
    seq = ("z", "yy", "hy")
    in_specs = (
        P(seq, "tp"),
        P(),
        P(None, "tp"),
        P(None, "tp"),
        P(None, "tp"),
        P(None, "tp"),
        P(None, "tp"),
        P(None, "tp"),
        P("tp"),
        P("tp"),
        P("tp"),
        P("tp"),
        P("tp", None),
        P("tp", None),
        P(),
    )
    out_specs = P((*seq, "tp"), None)
    return jax.shard_map(shards, mesh=cube, in_specs=in_specs, out_specs=out_specs, check_vma=False)
```

time: 126 us -> 104 us (0.83)
  waiting for transfers between devices: 26.3 us -> 13.9 us
  Pallas kernels: 23.1 us -> 16.8 us
  local copies, waits for them, and re-layouts: 5.1 us -> 0.04 us
  blocking collectives: 59.1 us -> 60.4 us
    all_to_all x2, waiting for transfers between devices: 25.3 us -> 12.7 us  [swap(): return lax.all_to_all(value, axis, 0, 0, tiled=True)]
    pallas_call x5 -> x6, Pallas kernels: 23.1 us -> 16.8 us  [begun(): run(*[pltpu.with_memory_space_constraint(a, spaces[id(spec)]) if id(spec)...]
    unnamed x12 -> x14, local copies, waits for them, and re-layouts: 5.1 us -> 0.04 us
    ppermute x1, starting transfers between devices: 1.29 us -> 3.96 us  [shards(): lax.ppermute(kv_win, ('z', 'yy', 'hy'), [(i, i + 1) for i in range(count...]
    all_to_all x2, blocking collectives: 37.9 us -> 40.4 us  [swap(): return lax.all_to_all(value, axis, 0, 0, tiled=True)]
    all_to_all x2, starting transfers between devices: 10.2 us -> 8.17 us  [swap(): return lax.all_to_all(value, axis, 0, 0, tiled=True)]
  transfers between devices with their start and end apart: 3 -> 3, of which waited for: 3 -> 3; matrix products, arithmetic and copies ran while one was open for 1% -> 0% of each run, Pallas kernels for 2% -> 4%
where the time goes in v2:
time: 104 us; the launch traced here: 103 us
  blocking collectives  60.4 us (58%)
  Pallas kernels  16.8 us (16%)
  waiting for transfers between devices  13.9 us (13%)
  starting transfers between devices  12.1 us (12%)
    all_to_all x2, blocking collectives, swap(): return lax.all_to_all(value, axis, 0, 0, tiled=True)  40.4 us
    all_gather x1, blocking collectives, shards(): lax.all_gather(tokens, 'tp', axis=0, tiled=True)  20 us
    pallas_call x6, Pallas kernels, begun(): run(*[pltpu.with_memory_space_constraint(a, spaces[id(spec)]) if id(spec)...  16.8 us
    all_to_all x2, waiting for transfers between devices, swap(): return lax.all_to_all(value, axis, 0, 0, tiled=True)  12.7 us
    all_to_all x2, starting transfers between devices, swap(): return lax.all_to_all(value, axis, 0, 0, tiled=True)  8.17 us
    ppermute x1, starting transfers between devices, shards(): lax.ppermute(kv_win, ('z', 'yy', 'hy'), [(i, i + 1) for i in range(count...  3.96 us
  transfers between devices with their start and end apart: 3, of which 3 were waited for; matrix products, arithmetic and copies ran while one was open for 0% of the time, Pallas kernels for 4%

profile of v2, /device:TPU:1, one launch (start us, length us, event | category | flops | bytes accessed | tf_op | source)
XLA Modules:
  0.0 103.4 jit_solution(16485055683317670790)
XLA Ops:
  0.0 20.0 %all_gather.3 = bf16[1024,256]{1,0:T(8,128)(2,1)S(1)} all-gather(bf16[128,256]{1,0:T(8,128)(2,1)} %param.15), channel_id=1, replica_groups=mesh['z'=8,'yy'=4,'hy'=2,'tp'=8] {'tp'}, dimensions={0}, use_global_device_ids=true | all-gather | bytes 589824 | tf_op jit(solution)/shard_map/all_gather | solution.py:276
  20.0 2.9 %shard_map.145 = (bf16[8,128,128]{2,1,0:T(8,128)(2,1)}, bf16[128,2048]{1,0:T(8,128)(2,1)S(1)}) custom-call(bf16[8,128,256]{2,1,0:T(8,128)(2,1)S(1)} %bitcast.10, f32[1,2048]{1,0:T(1,128)} %bitcast.17, bf16[2048,128]{1,0:T(8,128)(2,1)} %wk.1, bf16[2048,128]{1,0:T(8,128)(2,1)} %wv.1), custom_call_target="tpu_custom_call" | custom-call | tf_op jit(solution)/shard_map/pallas_call | solution.py:45
  22.8 3.4 %all-to-all-start.1 = ((bf16[8,128,128]{2,1,0:T(8,128)(2,1)}), bf16[8,128,128]{2,1,0:T(8,128)(2,1)S(1)}, u32[]{:S(2)}, u32[]{:S(2)}) async-start(bf16[8,128,128]{2,1,0:T(8,128)(2,1)} %get-tuple-element.14), calls=%async_computation.1 | async-start | bytes 524288 | tf_op jit(solution)/shard_map/all_to_all | solution.py:274
  26.3 0.0 copy-start.5
  26.3 2.6 %shard_map.146 = (bf16[8,2,64,128]{3,2,1,0:T(8,128)(2,1)S(1)}, bf16[128,128]{1,0:T(8,128)(2,1)S(1)}, bf16[128,128]{1,0:T(8,128)(2,1)S(1)}) custom-call(bf16[128,2048]{1,0:T(8,128)(2,1)S(1)} %get-tuple-element.12.normed_in, bf16[2048,128]{1,0:T(8,128)(2,1)} %wq.1, bf16[2048,128]{1,0:T(8,128)(2,1)} %wqw.1, bf16[64,2048]{1,0:T(8,128)(2,1)} %bitcast.15, ...), custom_call_target="tpu_custom_call" | custom-call | tf_op jit(solution)/shard_map/pallas_call | solution.py:45
  28.9 0.0 copy-start
  28.9 0.0 copy-start.3
  28.9 0.0 copy-start.4
  28.9 9.6 %all-to-all-done.1.kv = bf16[8,128,128]{2,1,0:T(8,128)(2,1)S(1)} async-done(((bf16[8,128,128]{2,1,0:T(8,128)(2,1)}), bf16[8,128,128]{2,1,0:T(8,128)(2,1)S(1)}, u32[]{:S(2)}, u32[]{:S(2)}) %all-to-all-start.1) | async-done | bytes 262176 | tf_op jit(solution)/shard_map/all_to_all | solution.py:274
  38.6 17.2 %all_to_all.20.q = bf16[16,64,128]{2,1,0:T(8,128)(2,1)S(1)} all-to-all(bf16[16,64,128]{2,1,0:T(8,128)(2,1)S(1)} %bitcast.11), channel_id=1, replica_groups=mesh['z'=8,'yy'=4,'hy'=2,'tp'=8] {'z','hy'}, dimensions={0} | all-to-all | bytes 524288 | tf_op jit(solution)/shard_map/all_to_all | solution.py:274
  55.8 0.0 copy-done.5
  55.8 0.0 copy-start.1
  55.8 0.0 copy-start.6
  55.8 8.7 %shard_map.147 = bf16[16,72,128]{2,1,0:T(8,128)(2,1)} custom-call(f32[2]{0:T(128)S(1)} %copy-done.5, bf16[16,64,128]{2,1,0:T(8,128)(2,1)S(1)} %all_to_all.20.q, bf16[8,128,128]{2,1,0:T(8,128)(2,1)S(1)} %all-to-all-done.1.kv), custom_call_target="tpu_custom_call" | custom-call | tf_op jit(solution)/shard_map/pallas_call | solution.py:45
  64.5 4.7 %all-to-all-start.2 = ((bf16[16,72,128]{2,1,0:T(8,128)(2,1)}), bf16[16,72,128]{2,1,0:T(8,128)(2,1)S(1)}, u32[]{:S(2)}, u32[]{:S(2)}) async-start(bf16[16,72,128]{2,1,0:T(8,128)(2,1)} %shard_map.147), calls=%async_computation.2 | async-start | bytes 589824 | tf_op jit(solution)/shard_map/all_to_all | solution.py:274
  69.2 4.0 %collective-permute-start = (bf16[128,128]{1,0:T(8,128)(2,1)S(1)}, bf16[128,128]{1,0:T(8,128)(2,1)S(1)}, u32[]{:S(2)}, u32[]{:S(2)}) collective-permute-start(bf16[128,128]{1,0:T(8,128)(2,1)S(1)} %get-tuple-element.16.own), channel_id=1, source_target_pairs={{0,8},{8,16},{16,24},{24,32},{32,40},{40,48},{48,56},{56,64},{64,7... | collective-permute-start | bytes 98312 | tf_op jit(solution)/shard_map/ppermute | solution.py:306
  73.2 1.2 %collective-permute-done.prev = bf16[128,128]{1,0:T(8,128)(2,1)S(1)} collective-permute-done((bf16[128,128]{1,0:T(8,128)(2,1)S(1)}, bf16[128,128]{1,0:T(8,128)(2,1)S(1)}, u32[]{:S(2)}, u32[]{:S(2)}) %collective-permute-start) | collective-permute-done | bytes 32800 | tf_op jit(solution)/shard_map/ppermute | solution.py:306
  74.4 0.0 copy-done
  74.4 0.0 copy-done.3
  74.4 0.0 copy-done.4
  74.4 1.3 %shard_map.148 = (bf16[128,2048]{1,0:T(8,128)(2,1)S(1)}, f32[128,128]{1,0:T(8,128)S(1)}) custom-call(f32[2]{0:T(128)S(1)} %copy-done.3, bf16[128,128]{1,0:T(8,128)(2,1)S(1)} %get-tuple-element.15.qw, bf16[128,128]{1,0:T(8,128)(2,1)S(1)} %collective-permute-done.prev, bf16[128,128]{1,0:T(8,128)(2,1)S(1)} %get-tuple-element.16.own, ...), custom_call_target="tpu_custom_call" | custom-call | tf_op jit(solution)/shard_map/pallas_call | solution.py:45
  75.7 3.1 %all-to-all-done.2.parts = bf16[16,72,128]{2,1,0:T(8,128)(2,1)S(1)} async-done(((bf16[16,72,128]{2,1,0:T(8,128)(2,1)}), bf16[16,72,128]{2,1,0:T(8,128)(2,1)S(1)}, u32[]{:S(2)}, u32[]{:S(2)}) %all-to-all-start.2) | async-done | bytes 294944 | tf_op jit(solution)/shard_map/all_to_all | solution.py:274
  78.8 0.0 copy-done.1
  78.8 0.0 copy-done.6
  78.8 0.4 shard_map.149
  79.2 0.0 copy-start.2
  79.2 23.3 %all_to_all.21.parts = bf16[8,16,4224]{2,1,0:T(8,128)(2,1)S(1)} all-to-all(bf16[8,16,4224]{2,1,0:T(8,128)(2,1)S(1)} %bitcast.9), channel_id=1, replica_groups=mesh['z'=8,'yy'=4,'hy'=2,'tp'=8] {'tp'}, dimensions={0} | all-to-all | bytes 2162688 | tf_op jit(solution)/shard_map/all_to_all | solution.py:274
  102.4 0.0 copy-done.2
  102.4 1.0 shard_map.150
Async XLA Ops:
  22.8 15.7 %all-to-all-start.1 = ((bf16[8,128,128]{2,1,0:T(8,128)(2,1)}), bf16[8,128,128]{2,1,0:T(8,128)(2,1)S(1)}, u32[]{:S(2)}, u32[]{:S(2)}) async-start(bf16[8,128,128]{2,1,0:T(8,128)(2,1)} %get-tuple-element.14), calls=%async_computation.1 | async-start | bytes 524288 | tf_op jit(solution)/shard_map/all_to_all | solution.py:274
  26.3 29.5 %copy-start.5 = (f32[2]{0:T(128)S(1)}, f32[2]{0:T(128)}, u32[]{:S(2)}) copy-start(f32[2]{0:T(128)} %bias.1) | copy-start | bytes 28
  28.9 45.5 %copy-start = (bf16[128,2048]{1,0:T(8,128)(2,1)S(1)}, bf16[128,2048]{1,0:T(8,128)(2,1)}, u32[]{:S(2)}) copy-start(bf16[128,2048]{1,0:T(8,128)(2,1)} %w_out.2) | copy-start | bytes 1572868
  28.9 45.4 %copy-start.3 = (f32[2]{0:T(128)S(1)}, f32[2]{0:T(128)}, u32[]{:S(2)}) copy-start(f32[2]{0:T(128)} %sinks.1) | copy-start | bytes 28
  28.9 45.4 %copy-start.4 = (f32[128]{0:T(128)S(1)}, f32[128]{0:T(128)}, u32[]{:S(2)}) copy-start(f32[128]{0:T(128)} %param.26) | copy-start | bytes 1540
  55.8 23.0 %copy-start.1 = (bf16[128,2048]{1,0:T(8,128)(2,1)S(1)}, bf16[128,2048]{1,0:T(8,128)(2,1)}, u32[]{:S(2)}) copy-start(bf16[128,2048]{1,0:T(8,128)(2,1)} %w_out.3) | copy-start | bytes 1572868
  55.8 23.0 %copy-start.6 = (f32[128]{0:T(128)S(1)}, f32[128]{0:T(128)}, u32[]{:S(2)}) copy-start(f32[128]{0:T(128)} %param.25) | copy-start | bytes 1540
  64.5 14.3 %all-to-all-start.2 = ((bf16[16,72,128]{2,1,0:T(8,128)(2,1)}), bf16[16,72,128]{2,1,0:T(8,128)(2,1)S(1)}, u32[]{:S(2)}, u32[]{:S(2)}) async-start(bf16[16,72,128]{2,1,0:T(8,128)(2,1)} %shard_map.147), calls=%async_computation.2 | async-start | bytes 589824 | tf_op jit(solution)/shard_map/all_to_all | solution.py:274
  69.2 5.2 %collective-permute-start = (bf16[128,128]{1,0:T(8,128)(2,1)S(1)}, bf16[128,128]{1,0:T(8,128)(2,1)S(1)}, u32[]{:S(2)}, u32[]{:S(2)}) collective-permute-start(bf16[128,128]{1,0:T(8,128)(2,1)S(1)} %get-tuple-element.16.own), channel_id=1, source_target_pairs={{0,8},{8,16},{16,24},{24,32},{32,40},{40,48},{48,56},{56,64},{64,7... | collective-permute-start | bytes 98312 | tf_op jit(solution)/shard_map/ppermute | solution.py:306
  79.2 23.3 %copy-start.2 = (f32[2048]{0:T(1024)S(1)}, f32[2048]{0:T(1024)}, u32[]{:S(2)}) copy-start(f32[2048]{0:T(1024)} %param.29) | copy-start | bytes 24580

commit v3 on v2

--- a/solution.py
+++ b/solution.py
@@ -13,7 +13,7 @@
 SW_WIDTH = 1024
 ROWS = 8
 TAIL = 8
-PIECES = 4
+PIECES = 1
 LOG2E = 1.4426950408889634
 SCALE = HEAD_DIM ** (-0.5)
 
@@ -81,19 +81,29 @@
     return ready
 
 
-def keys_kernel(tok, gain, wk, wv, kv_out, normed_out, *held):
-    ready = fetched((wk, wv, gain), held[:3], held[3])
+def keys_kernel(tok, gain, wk, wv, kv_out, normed_out, both, gains, sems):
+    half = wk.shape[1]
+    copies = [
+        pltpu.make_async_copy(source, holder, sems.at[i])
+        for i, (source, holder) in enumerate(
+            ((gain, gains), (wk, both.at[:, :half]), (wv, both.at[:, half:]))
+        )
+    ]
+    for copy in copies:
+        copy.start()
     parts = tok.shape[0]
     wide = [tok[i].astype(f32) for i in range(parts)]
     total = sum(jnp.sum(w * w, axis=1, keepdims=True) for w in wide)
     scale = lax.rsqrt(total / (parts * tok.shape[2]) + epsilon)
     step = tok.shape[2]
-    gains = ready(2)
+    copies[0].wait()
     for i, w in enumerate(wide):
         normed_out[:, i * step : (i + 1) * step] = (w * scale * gains[:, i * step : (i + 1) * step]).astype(bf16)
     normed = normed_out[...]
-    key = dot(normed, ready(0))
-    value = dot(normed, ready(1))
+    copies[1].wait()
+    copies[2].wait()
+    made = dot(normed, both[...])
+    key, value = made[:, :half], made[:, half:]
     first = lax.broadcasted_iota(jnp.int32, (TILE, TILE), 1) < HEAD_DIM
     heads = [
         jnp.where(first, key, pltpu.roll(value, HEAD_DIM, 1)).astype(bf16),
@@ -127,8 +137,11 @@
     after = jnp.where(c_i > r_i, 1.0, 0.0).astype(bf16)
     for j in range(blocks):
         cols = slice(j * TILE, (j + 1) * TILE)
-        keys[cols] = kv[j, :, :HEAD_DIM]
-        values[:, cols] = jnp.transpose(kv[j].astype(f32))[HEAD_DIM:].astype(bf16)
+        both = kv[j].astype(f32)
+        high, low = split(both[:, :HEAD_DIM] * (SCALE * LOG2E))
+        keys[cols, :HEAD_DIM] = high
+        keys[cols, HEAD_DIM:] = low
+        values[:, cols] = jnp.transpose(both)[HEAD_DIM:].astype(bf16)
 
     def clear(block, _):
         out[2 * block] = jnp.zeros(out.shape[1:], bf16)
@@ -137,47 +150,52 @@
 
     lax.fori_loop(0, row, clear, 0)
 
-    def block_step(block, masked):
-        query = jnp.concatenate([q[2 * block], q[2 * block + 1]], axis=1)
-        carry = [jnp.zeros((1, pair), f32)]
-
-        def open_tile(j):
-            s = dot(keys[j * TILE : (j + 2) * TILE], query) * (SCALE * LOG2E) + shift
+    def block_steps(steps):
+        queries = [jnp.concatenate([q[2 * b], q[2 * b + 1]], axis=1) for b, _ in steps]
+        queries = [jnp.concatenate([v, v], axis=0) for v in queries]
+        carry = [jnp.zeros((1, pair), f32) for _ in steps]
+
+        def open_tile(n, j):
+            s = dot(keys[j * TILE : (j + 2) * TILE], queries[n]) + shift
             soft = jnp.maximum(s, lax.log2(1.0 + jnp.exp2(jnp.minimum(s, 126.0))))
             rest = s - soft
-            if masked:
+            if steps[n][1]:
                 seen = (j * TILE + r_i) < (duo * pair + c_i)
                 soft = jnp.where(seen, soft, 0.0)
                 rest = jnp.where(seen, rest, -jnp.inf)
             return rest, soft[:1], dot(after, soft.astype(bf16))
 
-        def close_tile(j, rest, own, sums):
-            w = jnp.exp2(rest - (sums + carry[0]))
-            weight[j * TILE : (j + 2) * TILE] = w.astype(bf16)
-            carry[0] = carry[0] + (sums[:1] + own)
-
-        units = list(reversed(range(0, blocks, 2)))
-        opened = open_tile(units[0])
+        def close_tile(n, j, rest, own, sums):
+            w = jnp.exp2(rest - (sums + carry[n]))
+            weight[n, j * TILE : (j + 2) * TILE] = w.astype(bf16)
+            carry[n] = carry[n] + (sums[:1] + own)
+
+        units = [(n, j) for j in reversed(range(0, blocks, 2)) for n in range(len(steps))]
+        opened = open_tile(*units[0])
         for at, unit in enumerate(units):
-            following = open_tile(units[at + 1]) if at + 1 < len(units) else None
-            close_tile(unit, *opened)
+            following = open_tile(*units[at + 1]) if at + 1 < len(units) else None
+            close_tile(*unit, *opened)
             opened = following
-        acc = dot(values[...], weight[...])
-        high, low = split(carry[0])
-        tail = lax.broadcasted_iota(jnp.int32, (TAIL, pair), 0)
-        tail = jnp.where(tail == 0, high.astype(f32), jnp.where(tail == 1, low.astype(f32), 0.0))
-        for i in range(2):
-            cols = slice(i * TILE, (i + 1) * TILE)
-            out[2 * block + i, :HEAD_DIM] = acc[:, cols].astype(bf16)
-            out[2 * block + i, HEAD_DIM:] = tail[:, cols].astype(bf16)
-
-    block_step(row, True)
-
-    def later(block, _):
-        block_step(block, False)
+        for n in reversed(range(len(steps))):
+            block = steps[n][0]
+            acc = dot(values[...], weight[n])
+            high, low = split(carry[n])
+            tail = lax.broadcasted_iota(jnp.int32, (TAIL, pair), 0)
+            tail = jnp.where(tail == 0, high.astype(f32), jnp.where(tail == 1, low.astype(f32), 0.0))
+            for i in range(2):
+                cols = slice(i * TILE, (i + 1) * TILE)
+                out[2 * block + i, :HEAD_DIM] = acc[:, cols].astype(bf16)
+                out[2 * block + i, HEAD_DIM:] = tail[:, cols].astype(bf16)
+
+    last = out.shape[0] // 2 - 1
+    block_steps(((row, True), (jnp.minimum(row + 1, last), False)))
+
+    def later(step, _):
+        block = row + 2 + 2 * step
+        block_steps(((block, False), (jnp.minimum(block + 1, last), False)))
         return 0
 
-    lax.fori_loop(row + 1, out.shape[0] // 2, later, 0)
+    lax.fori_loop(0, lax.div(last - row, 2), later, 0)
 
 
 def window_kernel(sinks, qw, prev, own, w_out, gain, prod_out, ssq_out):
@@ -279,7 +297,6 @@
     def holders(arrays):
         return [pltpu.VMEM(a.shape, a.dtype) for a in arrays] + [pltpu.SemaphoreType.DMA((PIECES * len(arrays),))]
 
-    weights = (w_key_stick, w_value_stick)
     gain = pre_gain.reshape(1, width)
     kv_all, normed = call(
         keys_kernel,
@@ -288,8 +305,12 @@
             jax.ShapeDtypeStruct((tok_rows, width), bf16),
         ),
         [VM, HB, HB, HB],
-        scratch=holders(weights + (gain,)),
-    )(gathered, gain, *weights)
+        scratch=[
+            pltpu.VMEM((width, 2 * head_pair), bf16),
+            pltpu.VMEM((1, width), f32),
+            pltpu.SemaphoreType.DMA((3,)),
+        ],
+    )(gathered, gain, w_key_stick, w_value_stick)
     kv_row = swap(kv_all, ("yy", "hy"))
     weights = (w_query_stick, w_query_window, w_key_window.T, w_value_window.T)
     q_all, q_win, kv_win = call(
@@ -315,8 +336,8 @@
         jax.ShapeDtypeStruct((2 * nz, HEAD_DIM + TAIL, TILE), bf16),
         [SM, VM, VM],
         scratch=[
-            pltpu.VMEM((ROWS * TILE, 2 * TILE), bf16),
-            pltpu.VMEM((ROWS * TILE, HEAD_DIM), bf16),
+            pltpu.VMEM((2, ROWS * TILE, 2 * TILE), bf16),
+            pltpu.VMEM((ROWS * TILE, 2 * HEAD_DIM), bf16),
             pltpu.VMEM((HEAD_DIM, ROWS * TILE), bf16),
         ],
     )(stick_bias, q_col, kv_row)

time: 104 us -> 102 us (0.981)
  Pallas kernels: 16.8 us -> 14.8 us
    pallas_call x6, Pallas kernels: 16.8 us -> 14.8 us  [begun(): run(*[pltpu.with_memory_space_constraint(a, spaces[id(spec)]) if id(spec)...]
where the time goes in v3:
time: 102 us; the launch traced here: 101 us
  blocking collectives  60.4 us (59%)
  Pallas kernels  14.8 us (15%)
  waiting for transfers between devices  14 us (14%)
  starting transfers between devices  12.1 us (12%)
    all_to_all x2, blocking collectives, swap(): return lax.all_to_all(value, axis, 0, 0, tiled=True)  40.4 us
    all_gather x1, blocking collectives, shards(): lax.all_gather(tokens, 'tp', axis=0, tiled=True)  20 us
    pallas_call x6, Pallas kernels, begun(): run(*[pltpu.with_memory_space_constraint(a, spaces[id(spec)]) if id(spec)...  14.8 us
    all_to_all x2, waiting for transfers between devices, swap(): return lax.all_to_all(value, axis, 0, 0, tiled=True)  12.8 us
    all_to_all x2, starting transfers between devices, swap(): return lax.all_to_all(value, axis, 0, 0, tiled=True)  8.16 us
    ppermute x1, starting transfers between devices, shards(): lax.ppermute(kv_win, ('z', 'yy', 'hy'), [(i, i + 1) for i in range(count...  3.96 us
  transfers between devices with their start and end apart: 3, of which 3 were waited for; matrix products, arithmetic and copies ran while one was open for 0% of the time, Pallas kernels for 4%

profile of v3, /device:TPU:1, one launch (start us, length us, event | category | flops | bytes accessed | tf_op | source)
XLA Modules:
  0.0 101.4 jit_solution(3703953649875074811)
XLA Ops:
  0.0 20.0 %all_gather.3 = bf16[1024,256]{1,0:T(8,128)(2,1)S(1)} all-gather(bf16[128,256]{1,0:T(8,128)(2,1)} %param.15), channel_id=1, replica_groups=mesh['z'=8,'yy'=4,'hy'=2,'tp'=8] {'tp'}, dimensions={0}, use_global_device_ids=true | all-gather | bytes 589824 | tf_op jit(solution)/shard_map/all_gather | solution.py:294
  20.0 2.5 %shard_map.145 = (bf16[8,128,128]{2,1,0:T(8,128)(2,1)}, bf16[128,2048]{1,0:T(8,128)(2,1)S(1)}) custom-call(bf16[8,128,256]{2,1,0:T(8,128)(2,1)S(1)} %bitcast.10, f32[1,2048]{1,0:T(1,128)} %bitcast.17, bf16[2048,128]{1,0:T(8,128)(2,1)} %wk.1, bf16[2048,128]{1,0:T(8,128)(2,1)} %wv.1), custom_call_target="tpu_custom_call" | custom-call | tf_op jit(solution)/shard_map/pallas_call | solution.py:45
  22.5 3.4 %all-to-all-start.1 = ((bf16[8,128,128]{2,1,0:T(8,128)(2,1)}), bf16[8,128,128]{2,1,0:T(8,128)(2,1)S(1)}, u32[]{:S(2)}, u32[]{:S(2)}) async-start(bf16[8,128,128]{2,1,0:T(8,128)(2,1)} %get-tuple-element.14), calls=%async_computation.1 | async-start | bytes 524288 | tf_op jit(solution)/shard_map/all_to_all | solution.py:292
  25.9 0.0 copy-start.5
  25.9 2.5 %shard_map.146 = (bf16[8,2,64,128]{3,2,1,0:T(8,128)(2,1)S(1)}, bf16[128,128]{1,0:T(8,128)(2,1)S(1)}, bf16[128,128]{1,0:T(8,128)(2,1)S(1)}) custom-call(bf16[128,2048]{1,0:T(8,128)(2,1)S(1)} %get-tuple-element.12.normed_in, bf16[2048,128]{1,0:T(8,128)(2,1)} %wq.1, bf16[2048,128]{1,0:T(8,128)(2,1)} %wqw.1, bf16[64,2048]{1,0:T(8,128)(2,1)} %bitcast.15, ...), custom_call_target="tpu_custom_call" | custom-call | tf_op jit(solution)/shard_map/pallas_call | solution.py:45
  28.4 0.0 copy-start
  28.4 0.0 copy-start.3
  28.4 0.0 copy-start.4
  28.5 9.7 %all-to-all-done.1.kv = bf16[8,128,128]{2,1,0:T(8,128)(2,1)S(1)} async-done(((bf16[8,128,128]{2,1,0:T(8,128)(2,1)}), bf16[8,128,128]{2,1,0:T(8,128)(2,1)S(1)}, u32[]{:S(2)}, u32[]{:S(2)}) %all-to-all-start.1) | async-done | bytes 262176 | tf_op jit(solution)/shard_map/all_to_all | solution.py:292
  38.2 17.2 %all_to_all.20.q = bf16[16,64,128]{2,1,0:T(8,128)(2,1)S(1)} all-to-all(bf16[16,64,128]{2,1,0:T(8,128)(2,1)S(1)} %bitcast.11), channel_id=1, replica_groups=mesh['z'=8,'yy'=4,'hy'=2,'tp'=8] {'z','hy'}, dimensions={0} | all-to-all | bytes 524288 | tf_op jit(solution)/shard_map/all_to_all | solution.py:292
  55.4 0.0 copy-done.5
  55.4 0.0 copy-start.1
  55.4 0.0 copy-start.6
  55.4 7.1 %shard_map.147 = bf16[16,72,128]{2,1,0:T(8,128)(2,1)} custom-call(f32[2]{0:T(128)S(1)} %copy-done.5, bf16[16,64,128]{2,1,0:T(8,128)(2,1)S(1)} %all_to_all.20.q, bf16[8,128,128]{2,1,0:T(8,128)(2,1)S(1)} %all-to-all-done.1.kv), custom_call_target="tpu_custom_call" | custom-call | tf_op jit(solution)/shard_map/pallas_call | solution.py:45
  62.5 4.7 %all-to-all-start.2 = ((bf16[16,72,128]{2,1,0:T(8,128)(2,1)}), bf16[16,72,128]{2,1,0:T(8,128)(2,1)S(1)}, u32[]{:S(2)}, u32[]{:S(2)}) async-start(bf16[16,72,128]{2,1,0:T(8,128)(2,1)} %shard_map.147), calls=%async_computation.2 | async-start | bytes 589824 | tf_op jit(solution)/shard_map/all_to_all | solution.py:292
  67.2 4.0 %collective-permute-start = (bf16[128,128]{1,0:T(8,128)(2,1)S(1)}, bf16[128,128]{1,0:T(8,128)(2,1)S(1)}, u32[]{:S(2)}, u32[]{:S(2)}) collective-permute-start(bf16[128,128]{1,0:T(8,128)(2,1)S(1)} %get-tuple-element.16.own), channel_id=1, source_target_pairs={{0,8},{8,16},{16,24},{24,32},{32,40},{40,48},{48,56},{56,64},{64,7... | collective-permute-start | bytes 98312 | tf_op jit(solution)/shard_map/ppermute | solution.py:327
  71.2 1.2 %collective-permute-done.prev = bf16[128,128]{1,0:T(8,128)(2,1)S(1)} collective-permute-done((bf16[128,128]{1,0:T(8,128)(2,1)S(1)}, bf16[128,128]{1,0:T(8,128)(2,1)S(1)}, u32[]{:S(2)}, u32[]{:S(2)}) %collective-permute-start) | collective-permute-done | bytes 32800 | tf_op jit(solution)/shard_map/ppermute | solution.py:327
  72.4 0.0 copy-done
  72.4 0.0 copy-done.3
  72.4 0.0 copy-done.4
  72.4 1.3 %shard_map.148 = (bf16[128,2048]{1,0:T(8,128)(2,1)S(1)}, f32[128,128]{1,0:T(8,128)S(1)}) custom-call(f32[2]{0:T(128)S(1)} %copy-done.3, bf16[128,128]{1,0:T(8,128)(2,1)S(1)} %get-tuple-element.15.qw, bf16[128,128]{1,0:T(8,128)(2,1)S(1)} %collective-permute-done.prev, bf16[128,128]{1,0:T(8,128)(2,1)S(1)} %get-tuple-element.16.own, ...), custom_call_target="tpu_custom_call" | custom-call | tf_op jit(solution)/shard_map/pallas_call | solution.py:45
  73.7 3.1 %all-to-all-done.2.parts = bf16[16,72,128]{2,1,0:T(8,128)(2,1)S(1)} async-done(((bf16[16,72,128]{2,1,0:T(8,128)(2,1)}), bf16[16,72,128]{2,1,0:T(8,128)(2,1)S(1)}, u32[]{:S(2)}, u32[]{:S(2)}) %all-to-all-start.2) | async-done | bytes 294944 | tf_op jit(solution)/shard_map/all_to_all | solution.py:292
  76.8 0.0 copy-done.1
  76.8 0.0 copy-done.6
  76.8 0.4 shard_map.149
  77.2 0.0 copy-start.2
  77.2 23.2 %all_to_all.21.parts = bf16[8,16,4224]{2,1,0:T(8,128)(2,1)S(1)} all-to-all(bf16[8,16,4224]{2,1,0:T(8,128)(2,1)S(1)} %bitcast.9), channel_id=1, replica_groups=mesh['z'=8,'yy'=4,'hy'=2,'tp'=8] {'tp'}, dimensions={0} | all-to-all | bytes 2162688 | tf_op jit(solution)/shard_map/all_to_all | solution.py:292
  100.5 0.0 copy-done.2
  100.5 1.0 shard_map.150
Async XLA Ops:
  22.5 15.7 %all-to-all-start.1 = ((bf16[8,128,128]{2,1,0:T(8,128)(2,1)}), bf16[8,128,128]{2,1,0:T(8,128)(2,1)S(1)}, u32[]{:S(2)}, u32[]{:S(2)}) async-start(bf16[8,128,128]{2,1,0:T(8,128)(2,1)} %get-tuple-element.14), calls=%async_computation.1 | async-start | bytes 524288 | tf_op jit(solution)/shard_map/all_to_all | solution.py:292
  25.9 29.5 %copy-start.5 = (f32[2]{0:T(128)S(1)}, f32[2]{0:T(128)}, u32[]{:S(2)}) copy-start(f32[2]{0:T(128)} %bias.1) | copy-start | bytes 28
  28.4 44.0 %copy-start = (bf16[128,2048]{1,0:T(8,128)(2,1)S(1)}, bf16[128,2048]{1,0:T(8,128)(2,1)}, u32[]{:S(2)}) copy-start(bf16[128,2048]{1,0:T(8,128)(2,1)} %w_out.2) | copy-start | bytes 1572868
  28.4 44.0 %copy-start.3 = (f32[2]{0:T(128)S(1)}, f32[2]{0:T(128)}, u32[]{:S(2)}) copy-start(f32[2]{0:T(128)} %sinks.1) | copy-start | bytes 28
  28.4 44.0 %copy-start.4 = (f32[128]{0:T(128)S(1)}, f32[128]{0:T(128)}, u32[]{:S(2)}) copy-start(f32[128]{0:T(128)} %param.26) | copy-start | bytes 1540
  55.4 21.4 %copy-start.1 = (bf16[128,2048]{1,0:T(8,128)(2,1)S(1)}, bf16[128,2048]{1,0:T(8,128)(2,1)}, u32[]{:S(2)}) copy-start(bf16[128,2048]{1,0:T(8,128)(2,1)} %w_out.3) | copy-start | bytes 1572868
  55.4 21.4 %copy-start.6 = (f32[128]{0:T(128)S(1)}, f32[128]{0:T(128)}, u32[]{:S(2)}) copy-start(f32[128]{0:T(128)} %param.25) | copy-start | bytes 1540
  62.5 14.3 %all-to-all-start.2 = ((bf16[16,72,128]{2,1,0:T(8,128)(2,1)}), bf16[16,72,128]{2,1,0:T(8,128)(2,1)S(1)}, u32[]{:S(2)}, u32[]{:S(2)}) async-start(bf16[16,72,128]{2,1,0:T(8,128)(2,1)} %shard_map.147), calls=%async_computation.2 | async-start | bytes 589824 | tf_op jit(solution)/shard_map/all_to_all | solution.py:292
  67.2 5.2 %collective-permute-start = (bf16[128,128]{1,0:T(8,128)(2,1)S(1)}, bf16[128,128]{1,0:T(8,128)(2,1)S(1)}, u32[]{:S(2)}, u32[]{:S(2)}) collective-permute-start(bf16[128,128]{1,0:T(8,128)(2,1)S(1)} %get-tuple-element.16.own), channel_id=1, source_target_pairs={{0,8},{8,16},{16,24},{24,32},{32,40},{40,48},{48,56},{56,64},{64,7... | collective-permute-start | bytes 98312 | tf_op jit(solution)/shard_map/ppermute | solution.py:327
  77.2 23.3 %copy-start.2 = (f32[2048]{0:T(1024)S(1)}, f32[2048]{0:T(1024)}, u32[]{:S(2)}) copy-start(f32[2048]{0:T(1024)} %param.29) | copy-start | bytes 24580

commit v4 on v3

--- a/solution.py
+++ b/solution.py
@@ -18,6 +18,7 @@
 SCALE = HEAD_DIM ** (-0.5)
 
 epsilon = 1e-06
+TP = ("x", "core")
 f32 = jnp.float32
 bf16 = jnp.bfloat16
 
@@ -198,7 +199,7 @@
     lax.fori_loop(0, lax.div(last - row, 2), later, 0)
 
 
-def window_kernel(sinks, qw, prev, own, w_out, gain, prod_out, ssq_out):
+def window_kernel(sinks, qw, prev, own, w_out, gain, keep, send):
     lane = lax.broadcasted_iota(jnp.int32, (TILE, TILE), 1)
     first = lane < HEAD_DIM
     block = lax.axis_index("z") + lax.axis_index("yy") + lax.axis_index("hy")
@@ -220,15 +221,28 @@
     weights = (powers / total).astype(bf16)
     mixed = dot(weights, pair)
     result = jnp.where(first, pltpu.roll(mixed[:TILE], HEAD_DIM, 1), mixed[TILE:]).astype(bf16).astype(f32)
-    ssq_out[...] = jnp.broadcast_to(jnp.sum(result * result, axis=1, keepdims=True), (TILE, TILE))
-    scaled = (result * gain[...]).astype(bf16)
-    prod_out[...] = dot(scaled, w_out[...]).astype(bf16)
-
-
-def combine_kernel(parts, gain, w_out, prod_w, ssq_w, out):
+    share(result, gain, w_out, keep, send)
+
+
+def share(result, gain, w_out, keep, send):
+    width = w_out.shape[1]
+    ssq = jnp.sum(result * result, axis=1, keepdims=True)
+    high, low = split(jnp.broadcast_to(ssq, (TILE, TILE)))
+    lane = lax.broadcasted_iota(jnp.int32, (TILE, TILE), 1)
+    squares = jnp.where(lane == 0, high.astype(f32), low.astype(f32))
+    product = dot((result * gain[...]).astype(bf16), w_out[...])
+    own = lax.axis_index("core") == 0
+    rows = keep.shape[1]
+    for value, cols in ((product, slice(0, width)), (squares, slice(width, width + TILE))):
+        for at in range(keep.shape[0]):
+            even = value[2 * at * rows : (2 * at + 1) * rows]
+            odd = value[(2 * at + 1) * rows : (2 * at + 2) * rows]
+            keep[at, :, cols] = jnp.where(own, even, odd).astype(bf16)
+            send[at, :, cols] = jnp.where(own, odd, even).astype(bf16)
+
+
+def combine_kernel(parts, gain, w_out, keep, send):
     count = parts.shape[0] // 2
-    width = w_out.shape[1]
-    lane = lax.broadcasted_iota(jnp.int32, (TILE, TILE), 1)
     heads = []
     for h in range(2):
         later = jnp.zeros((1, TILE), f32)
@@ -240,18 +254,22 @@
             later = later + tail[0:1] + tail[1:2]
         heads.append(total)
     result = jnp.transpose(jnp.concatenate(heads, axis=0))
-    result = result.astype(bf16).astype(f32)
-    ssq = jnp.sum(result * result, axis=1, keepdims=True)
-    scaled = (result * gain[...]).astype(bf16)
-    out[:, :width] = dot(scaled, w_out[...]).astype(bf16)
-    out[:, width : 2 * width] = prod_w[...]
-    high_s, low_s = split(jnp.broadcast_to(ssq, (TILE, TILE)))
-    high_w, low_w = split(ssq_w[...])
-    out[:, 2 * width :] = jnp.where(
-        lane == 0,
-        high_s.astype(f32),
-        jnp.where(lane == 1, low_s.astype(f32), jnp.where(lane == 2, high_w.astype(f32), low_w.astype(f32))),
-    ).astype(bf16)
+    share(result.astype(bf16).astype(f32), gain, w_out, keep, send)
+
+
+def pairs_kernel(keep_s, came_s, keep_w, came_w, out):
+    width = keep_s.shape[2] - TILE
+    lane = lax.broadcasted_iota(jnp.int32, (keep_s.shape[1], TILE), 1)
+    for at in range(out.shape[0]):
+        parts = []
+        for n, (keep, came) in enumerate(((keep_s, came_s), (keep_w, came_w))):
+            both = keep[at].astype(f32) + came[at].astype(f32)
+            out[at, :, n * width : (n + 1) * width] = both[:, :width].astype(bf16)
+            parts += split(both[:, width : width + 1] + both[:, width + 1 : width + 2])
+        tail = parts[-1].astype(f32)
+        for n in reversed(range(len(parts) - 1)):
+            tail = jnp.where(lane == n, parts[n].astype(f32), tail)
+        out[at, :, 2 * width :] = tail.astype(bf16)
 
 
 def final_kernel(parts, gain, out):
@@ -285,13 +303,13 @@
     post_gain,
 ):
     tok_rows, feats = tokens.shape
-    nz, ntp = lax.axis_size("z"), lax.axis_size("tp")
+    nz, ntp = lax.axis_size("z"), lax.axis_size(TP)
     width = ntp * feats
 
     def swap(value, axis):
         return lax.all_to_all(value, axis, 0, 0, tiled=True)
 
-    gathered = lax.all_gather(tokens, "tp", axis=0, tiled=True).reshape(ntp, tok_rows, feats)
+    gathered = lax.all_gather(tokens, TP, axis=0, tiled=True).reshape(ntp, tok_rows, feats)
     head_pair = w_key_stick.shape[1]
 
     def holders(arrays):
@@ -326,11 +344,16 @@
     count = nz * ROWS
     previous = lax.ppermute(kv_win, ("z", "yy", "hy"), [(i, i + 1) for i in range(count - 1)])
     q_col = swap(q_all.reshape(2 * nz, HEAD_DIM, tok_rows), ("z", "hy"))
-    prod_w, ssq_w = call(
-        window_kernel,
-        (jax.ShapeDtypeStruct((tok_rows, width), bf16), jax.ShapeDtypeStruct((tok_rows, TILE), f32)),
-        [SM] + [VM] * 5,
-    )(sinks, q_win, previous, kv_win, w_out_window, window_gain.reshape(1, -1))
+    rows = tok_rows // ntp
+    halves = (jax.ShapeDtypeStruct((ntp // 2, rows, width + TILE), bf16),) * 2
+    keep_w, send_w = call(window_kernel, halves, [SM] + [VM] * 5)(
+        sinks, q_win, previous, kv_win, w_out_window, window_gain.reshape(1, -1)
+    )
+
+    def to_other_core(value):
+        return lax.ppermute(value, "core", [(0, 1), (1, 0)])
+
+    came_w = to_other_core(send_w)
     partial = call(
         stick_kernel,
         jax.ShapeDtypeStruct((2 * nz, HEAD_DIM + TAIL, TILE), bf16),
@@ -342,34 +365,38 @@
         ],
     )(stick_bias, q_col, kv_row)
     returned = swap(partial, ("z", "hy"))
+    keep_s, send_s = call(combine_kernel, halves, [VM] * 3)(returned, stick_gain.reshape(1, -1), w_out_stick)
+    came_s = to_other_core(send_s)
     sending = call(
-        combine_kernel, jax.ShapeDtypeStruct((tok_rows, 2 * width + TILE), bf16), [VM] * 5
-    )(returned, stick_gain.reshape(1, -1), w_out_stick, prod_w, ssq_w)
-    arrived = swap(sending.reshape(ntp, tok_rows // ntp, 2 * width + TILE), "tp")
+        pairs_kernel, jax.ShapeDtypeStruct((ntp // 2, rows, 2 * width + TILE), bf16), [VM] * 4
+    )(keep_s, came_s, keep_w, came_w)
+    arrived = swap(sending, "x")
     return call(
-        final_kernel, jax.ShapeDtypeStruct((tok_rows // ntp, width), bf16), [VM, VM], keep=False
+        final_kernel, jax.ShapeDtypeStruct((rows, width), bf16), [VM, VM], keep=False
     )(arrived, post_gain.reshape(1, width))
 
 
 def solution(mesh):
-    cube = Mesh(mesh.devices.reshape(-1, ROWS // 2, 2, mesh.devices.shape[-1]), ("z", "yy", "hy", "tp"))
+    cube = Mesh(
+        mesh.devices.reshape(-1, ROWS // 2, 2, mesh.devices.shape[-1] // 2, 2), ("z", "yy", "hy", "x", "core")
+    )
     seq = ("z", "yy", "hy")
     in_specs = (
-        P(seq, "tp"),
+        P(seq, TP),
         P(),
-        P(None, "tp"),
-        P(None, "tp"),
-        P(None, "tp"),
-        P(None, "tp"),
-        P(None, "tp"),
-        P(None, "tp"),
-        P("tp"),
-        P("tp"),
-        P("tp"),
-        P("tp"),
-        P("tp", None),
-        P("tp", None),
+        P(None, TP),
+        P(None, TP),
+        P(None, TP),
+        P(None, TP),
+        P(None, TP),
+        P(None, TP),
+        P(TP),
+        P(TP),
+        P(TP),
+        P(TP),
+        P(TP, None),
+        P(TP, None),
         P(),
     )
-    out_specs = P((*seq, "tp"), None)
+    out_specs = P((*seq, *TP), None)
     return jax.shard_map(shards, mesh=cube, in_specs=in_specs, out_specs=out_specs, check_vma=False)

time: 102 us -> 99.2 us (0.973)
  blocking collectives: 60.4 us -> 49.6 us
  starting transfers between devices: 12.1 us -> 20.5 us
  waiting for transfers between devices: 14 us -> 12.1 us
    all_to_all x2, blocking collectives: 40.4 us -> 29.6 us  [swap(): return lax.all_to_all(value, axis, 0, 0, tiled=True)]
    ppermute x0 -> x2, starting transfers between devices: none -> 8.28 us  [to_other_core(): return lax.ppermute(value, 'core', [(0, 1), (1, 0)])]
    all_to_all x2, waiting for transfers between devices: 12.8 us -> 9.77 us  [swap(): return lax.all_to_all(value, axis, 0, 0, tiled=True)]
    ppermute x0 -> x2, waiting for transfers between devices: none -> 1.16 us  [to_other_core(): return lax.ppermute(value, 'core', [(0, 1), (1, 0)])]
    pallas_call x6 -> x7, Pallas kernels: 14.8 us -> 15 us  [begun(): run(*[pltpu.with_memory_space_constraint(a, spaces[id(spec)]) if id(spec)...]
  transfers between devices with their start and end apart: 3 -> 5, of which waited for: 3 -> 3; matrix products, arithmetic and copies ran while one was open for 0% -> 0% of each run, Pallas kernels for 4% -> 4%
where the time goes in v4:
time: 99.2 us; the launch traced here: 98 us
  blocking collectives  49.6 us (50%)
  starting transfers between devices  20.5 us (21%)
  Pallas kernels  15 us (15%)
  waiting for transfers between devices  12.1 us (12%)
    all_to_all x2, blocking collectives, swap(): return lax.all_to_all(value, axis, 0, 0, tiled=True)  29.6 us
    all_gather x1, blocking collectives, shards(): lax.all_gather(tokens, TP, axis=0, tiled=True).reshape(ntp, tok_rows, feats)  20 us
    pallas_call x7, Pallas kernels, begun(): run(*[pltpu.with_memory_space_constraint(a, spaces[id(spec)]) if id(spec)...  15 us
    all_to_all x2, waiting for transfers between devices, swap(): return lax.all_to_all(value, axis, 0, 0, tiled=True)  9.77 us
    all_to_all x2, starting transfers between devices, swap(): return lax.all_to_all(value, axis, 0, 0, tiled=True)  8.3 us
    ppermute x2, starting transfers between devices, to_other_core(): return lax.ppermute(value, 'core', [(0, 1), (1, 0)])  8.28 us
    ppermute x1, starting transfers between devices, shards(): lax.ppermute(kv_win, ('z', 'yy', 'hy'), [(i, i + 1) for i in range(count...  3.96 us
  transfers between devices with their start and end apart: 5, of which 3 were waited for; matrix products, arithmetic and copies ran while one was open for 0% of the time, Pallas kernels for 4%

profile of v4, /device:TPU:1, one launch (start us, length us, event | category | flops | bytes accessed | tf_op | source)
XLA Modules:
  0.0 98.0 jit_solution(7633090570594189274)
XLA Ops:
  0.0 20.0 %all_gather.3 = bf16[1024,256]{1,0:T(8,128)(2,1)S(1)} all-gather(bf16[128,256]{1,0:T(8,128)(2,1)} %param.15), channel_id=1, replica_groups=mesh['z'=8,'yy'=4,'hy'=2,'x'=4,'core'=2] {'x','core'}, dimensions={0}, use_global_device_ids=true | all-gather | bytes 589824 | tf_op jit(solution)/shard_map/all_gather | solution.py:312
  20.0 2.4 %shard_map.145 = (bf16[8,128,128]{2,1,0:T(8,128)(2,1)}, bf16[128,2048]{1,0:T(8,128)(2,1)S(1)}) custom-call(bf16[8,128,256]{2,1,0:T(8,128)(2,1)S(1)} %bitcast.8, f32[1,2048]{1,0:T(1,128)} %bitcast.15, bf16[2048,128]{1,0:T(8,128)(2,1)} %wk.1, bf16[2048,128]{1,0:T(8,128)(2,1)} %wv.1), custom_call_target="tpu_custom_call" | custom-call | tf_op jit(solution)/shard_map/pallas_call | solution.py:46
  22.4 3.4 %all-to-all-start.1 = ((bf16[8,128,128]{2,1,0:T(8,128)(2,1)}), bf16[8,128,128]{2,1,0:T(8,128)(2,1)S(1)}, u32[]{:S(2)}, u32[]{:S(2)}) async-start(bf16[8,128,128]{2,1,0:T(8,128)(2,1)} %get-tuple-element.16), calls=%async_computation.1 | async-start | bytes 524288 | tf_op jit(solution)/shard_map/all_to_all | solution.py:310
  25.9 2.5 %shard_map.146 = (bf16[8,2,64,128]{3,2,1,0:T(8,128)(2,1)S(1)}, bf16[128,128]{1,0:T(8,128)(2,1)S(1)}, bf16[128,128]{1,0:T(8,128)(2,1)S(1)}) custom-call(bf16[128,2048]{1,0:T(8,128)(2,1)S(1)} %get-tuple-element.14.normed_in, bf16[2048,128]{1,0:T(8,128)(2,1)} %wq.1, bf16[2048,128]{1,0:T(8,128)(2,1)} %wqw.1, bf16[64,2048]{1,0:T(8,128)(2,1)} %bitcast.13, ...), custom_call_target="tpu_custom_call" | custom-call | tf_op jit(solution)/shard_map/pallas_call | solution.py:46
  28.4 9.8 %all-to-all-done.1.kv = bf16[8,128,128]{2,1,0:T(8,128)(2,1)S(1)} async-done(((bf16[8,128,128]{2,1,0:T(8,128)(2,1)}), bf16[8,128,128]{2,1,0:T(8,128)(2,1)S(1)}, u32[]{:S(2)}, u32[]{:S(2)}) %all-to-all-start.1) | async-done | bytes 262176 | tf_op jit(solution)/shard_map/all_to_all | solution.py:310
  38.2 0.0 copy-start.5
  38.2 17.3 %all_to_all.20.q = bf16[16,64,128]{2,1,0:T(8,128)(2,1)S(1)} all-to-all(bf16[16,64,128]{2,1,0:T(8,128)(2,1)S(1)} %bitcast.9), channel_id=1, replica_groups=mesh['z'=8,'yy'=4,'hy'=2,'x'=4,'core'=2] {'z','hy'}, dimensions={0} | all-to-all | bytes 524288 | tf_op jit(solution)/shard_map/all_to_all | solution.py:310
  55.5 0.0 copy-done.5
  55.5 0.0 copy-start
  55.5 7.1 %shard_map.147 = bf16[16,72,128]{2,1,0:T(8,128)(2,1)} custom-call(f32[2]{0:T(128)S(1)} %copy-done.5, bf16[16,64,128]{2,1,0:T(8,128)(2,1)S(1)} %all_to_all.20.q, bf16[8,128,128]{2,1,0:T(8,128)(2,1)S(1)} %all-to-all-done.1.kv), custom_call_target="tpu_custom_call" | custom-call | tf_op jit(solution)/shard_map/pallas_call | solution.py:46
  62.6 0.0 copy-start.1
  62.6 4.9 %all-to-all-start.2 = ((bf16[16,72,128]{2,1,0:T(8,128)(2,1)}), bf16[16,72,128]{2,1,0:T(8,128)(2,1)S(1)}, u32[]{:S(2)}, u32[]{:S(2)}) async-start(bf16[16,72,128]{2,1,0:T(8,128)(2,1)} %shard_map.147), calls=%async_computation.2 | async-start | bytes 589824 | tf_op jit(solution)/shard_map/all_to_all | solution.py:310
  67.5 4.0 %collective-permute-start.1 = (bf16[128,128]{1,0:T(8,128)(2,1)S(1)}, bf16[128,128]{1,0:T(8,128)(2,1)S(1)}, u32[]{:S(2)}, u32[]{:S(2)}) collective-permute-start(bf16[128,128]{1,0:T(8,128)(2,1)S(1)} %get-tuple-element.20.own), channel_id=1, source_target_pairs={{0,8},{8,16},{16,24},{24,32},{32,40},{40,48},{48,56},{56,64},{64,7... | collective-permute-start | bytes 98312 | tf_op jit(solution)/shard_map/ppermute | solution.py:345
  71.5 1.2 %collective-permute-done.1.prev = bf16[128,128]{1,0:T(8,128)(2,1)S(1)} collective-permute-done((bf16[128,128]{1,0:T(8,128)(2,1)S(1)}, bf16[128,128]{1,0:T(8,128)(2,1)S(1)}, u32[]{:S(2)}, u32[]{:S(2)}) %collective-permute-start.1) | collective-permute-done | bytes 32800 | tf_op jit(solution)/shard_map/ppermute | solution.py:345
  72.7 0.0 copy-done
  72.7 0.6 copy-done.3
  73.3 0.0 copy-done.4
  73.3 1.3 %shard_map.149 = (bf16[4,16,2176]{2,1,0:T(8,128)(2,1)S(1)}, bf16[4,16,2176]{2,1,0:T(8,128)(2,1)S(1)}) custom-call(f32[2]{0:T(128)S(1)} %copy-done.3, bf16[128,128]{1,0:T(8,128)(2,1)S(1)} %get-tuple-element.19.qw, bf16[128,128]{1,0:T(8,128)(2,1)S(1)} %collective-permute-done.1.prev, bf16[128,128]{1,0:T(8,128)(2,1)S(1)} %get-tuple-element.20.own, ...), custom_call_target="tpu_custom_call" | custom-call | tf_op jit(solution)/shard_map/pallas_call | solution.py:46
  74.7 0.0 copy-start.6
  74.7 4.4 %collective-permute-start.2 = (bf16[4,16,2176]{2,1,0:T(8,128)(2,1)S(1)}, bf16[4,16,2176]{2,1,0:T(8,128)(2,1)S(1)}, u32[]{:S(2)}, u32[]{:S(2)}) collective-permute-start(bf16[4,16,2176]{2,1,0:T(8,128)(2,1)S(1)} %get-tuple-element.22), channel_id=1, source_target_pairs={{0,1},{1,0},{2,3},{3,2},{4,5},{5,4},{6,7},{7,6},{8,9},{9,8},{10,11... | collective-permute-start | bytes 835592 | tf_op jit(solution)/shard_map/ppermute | solution.py:354
  79.1 0.0 all-to-all-done.2.parts
  79.1 0.0 copy-done.1
  79.1 0.0 copy-done.6
  79.1 0.4 shard_map.148
  79.5 3.9 %collective-permute-start = (bf16[4,16,2176]{2,1,0:T(8,128)(2,1)S(1)}, bf16[4,16,2176]{2,1,0:T(8,128)(2,1)S(1)}, u32[]{:S(2)}, u32[]{:S(2)}) collective-permute-start(bf16[4,16,2176]{2,1,0:T(8,128)(2,1)S(1)} %get-tuple-element.18), channel_id=1, source_target_pairs={{0,1},{1,0},{2,3},{3,2},{4,5},{5,4},{6,7},{7,6},{8,9},{9,8},{10,11... | collective-permute-start | bytes 835592 | tf_op jit(solution)/shard_map/ppermute | solution.py:354
  83.4 0.0 collective-permute-done.2.came_w
  83.4 1.2 %collective-permute-done.came_s = bf16[4,16,2176]{2,1,0:T(8,128)(2,1)S(1)} collective-permute-done((bf16[4,16,2176]{2,1,0:T(8,128)(2,1)S(1)}, bf16[4,16,2176]{2,1,0:T(8,128)(2,1)S(1)}, u32[]{:S(2)}, u32[]{:S(2)}) %collective-permute-start) | collective-permute-done | bytes 278560 | tf_op jit(solution)/shard_map/ppermute | solution.py:354
  84.6 0.3 shard_map.150
  84.8 0.0 copy-start.2
  84.9 12.3 %all_to_all.21.parts = bf16[4,16,4224]{2,1,0:T(8,128)(2,1)S(1)} all-to-all(bf16[4,16,4224]{2,1,0:T(8,128)(2,1)S(1)} %shard_map.150), channel_id=1, replica_groups=mesh['z'=8,'yy'=4,'hy'=2,'x'=4,'core'=2] {'x'}, dimensions={0} | all-to-all | bytes 1081344 | tf_op jit(solution)/shard_map/all_to_all | solution.py:310
  97.1 0.0 copy-done.2
  97.1 0.9 shard_map.151
  (2 shorter events, 0.0 us)
Async XLA Ops:
  22.4 15.7 %all-to-all-start.1 = ((bf16[8,128,128]{2,1,0:T(8,128)(2,1)}), bf16[8,128,128]{2,1,0:T(8,128)(2,1)S(1)}, u32[]{:S(2)}, u32[]{:S(2)}) async-start(bf16[8,128,128]{2,1,0:T(8,128)(2,1)} %get-tuple-element.16), calls=%async_computation.1 | async-start | bytes 524288 | tf_op jit(solution)/shard_map/all_to_all | solution.py:310
  38.2 17.3 %copy-start.5 = (f32[2]{0:T(128)S(1)}, f32[2]{0:T(128)}, u32[]{:S(2)}) copy-start(f32[2]{0:T(128)} %bias.1) | copy-start | bytes 28
  55.5 17.2 %copy-start = (bf16[128,2048]{1,0:T(8,128)(2,1)S(1)}, bf16[128,2048]{1,0:T(8,128)(2,1)}, u32[]{:S(2)}) copy-start(bf16[128,2048]{1,0:T(8,128)(2,1)} %w_out.3) | copy-start | bytes 1572868
  62.6 16.5 %copy-start.1 = (bf16[128,2048]{1,0:T(8,128)(2,1)S(1)}, bf16[128,2048]{1,0:T(8,128)(2,1)}, u32[]{:S(2)}) copy-start(bf16[128,2048]{1,0:T(8,128)(2,1)} %w_out.2) | copy-start | bytes 1572868
  62.6 16.5 %all-to-all-start.2 = ((bf16[16,72,128]{2,1,0:T(8,128)(2,1)}), bf16[16,72,128]{2,1,0:T(8,128)(2,1)S(1)}, u32[]{:S(2)}, u32[]{:S(2)}) async-start(bf16[16,72,128]{2,1,0:T(8,128)(2,1)} %shard_map.147), calls=%async_computation.2 | async-start | bytes 589824 | tf_op jit(solution)/shard_map/all_to_all | solution.py:310
  67.5 5.2 %collective-permute-start.1 = (bf16[128,128]{1,0:T(8,128)(2,1)S(1)}, bf16[128,128]{1,0:T(8,128)(2,1)S(1)}, u32[]{:S(2)}, u32[]{:S(2)}) collective-permute-start(bf16[128,128]{1,0:T(8,128)(2,1)S(1)} %get-tuple-element.20.own), channel_id=1, source_target_pairs={{0,8},{8,16},{16,24},{24,32},{32,40},{40,48},{48,56},{56,64},{64,7... | collective-permute-start | bytes 98312 | tf_op jit(solution)/shard_map/ppermute | solution.py:345
  72.7 0.7 copy-start.3
  72.7 0.7 copy-start.4
  74.7 4.5 %copy-start.6 = (f32[128]{0:T(128)S(1)}, f32[128]{0:T(128)}, u32[]{:S(2)}) copy-start(f32[128]{0:T(128)} %param.25) | copy-start | bytes 1540
  74.7 8.7 %collective-permute-start.2 = (bf16[4,16,2176]{2,1,0:T(8,128)(2,1)S(1)}, bf16[4,16,2176]{2,1,0:T(8,128)(2,1)S(1)}, u32[]{:S(2)}, u32[]{:S(2)}) collective-permute-start(bf16[4,16,2176]{2,1,0:T(8,128)(2,1)S(1)} %get-tuple-element.22), channel_id=1, source_target_pairs={{0,1},{1,0},{2,3},{3,2},{4,5},{5,4},{6,7},{7,6},{8,9},{9,8},{10,11... | collective-permute-start | bytes 835592 | tf_op jit(solution)/shard_map/ppermute | solution.py:354
  79.5 5.0 %collective-permute-start = (bf16[4,16,2176]{2,1,0:T(8,128)(2,1)S(1)}, bf16[4,16,2176]{2,1,0:T(8,128)(2,1)S(1)}, u32[]{:S(2)}, u32[]{:S(2)}) collective-permute-start(bf16[4,16,2176]{2,1,0:T(8,128)(2,1)S(1)} %get-tuple-element.18), channel_id=1, source_target_pairs={{0,1},{1,0},{2,3},{3,2},{4,5},{5,4},{6,7},{7,6},{8,9},{9,8},{10,11... | collective-permute-start | bytes 835592 | tf_op jit(solution)/shard_map/ppermute | solution.py:354
  84.8 12.3 %copy-start.2 = (f32[2048]{0:T(1024)S(1)}, f32[2048]{0:T(1024)}, u32[]{:S(2)}) copy-start(f32[2048]{0:T(1024)} %param.29) | copy-start | bytes 24580

commit v5 on v4

--- a/solution.py
+++ b/solution.py
@@ -13,7 +13,6 @@
 SW_WIDTH = 1024
 ROWS = 8
 TAIL = 8
-PIECES = 1
 LOG2E = 1.4426950408889634
 SCALE = HEAD_DIM ** (-0.5)
 
@@ -62,49 +61,51 @@
     return high, (value - high.astype(f32)).astype(bf16)
 
 
-def fetched(sources, holders, sems):
-    copies = []
-    for source, holder in zip(sources, holders):
-        step = source.shape[0] // PIECES if source.shape[0] % (8 * PIECES) == 0 else source.shape[0]
-        copies.append([])
-        for at in range(0, source.shape[0], step):
-            piece = pl.ds(at, step)
-            number = sum(map(len, copies))
-            copies[-1].append(pltpu.make_async_copy(source.at[piece], holder.at[piece], sems.at[number]))
-    for copy in sum(copies, []):
-        copy.start()
-
-    def ready(at):
-        for copy in copies[at]:
-            copy.wait()
-        return holders[at][...]
-
-    return ready
-
-
-def keys_kernel(tok, gain, wk, wv, kv_out, normed_out, both, gains, sems):
-    half = wk.shape[1]
-    copies = [
-        pltpu.make_async_copy(source, holder, sems.at[i])
-        for i, (source, holder) in enumerate(
-            ((gain, gains), (wk, both.at[:, :half]), (wv, both.at[:, half:]))
-        )
-    ]
+def fetched(sources, targets, sems):
+    copies = [pltpu.make_async_copy(s, t, sems.at[i]) for i, (s, t) in enumerate(zip(sources, targets))]
     for copy in copies:
         copy.start()
-    parts = tok.shape[0]
-    wide = [tok[i].astype(f32) for i in range(parts)]
-    total = sum(jnp.sum(w * w, axis=1, keepdims=True) for w in wide)
-    scale = lax.rsqrt(total / (parts * tok.shape[2]) + epsilon)
-    step = tok.shape[2]
-    copies[0].wait()
-    for i, w in enumerate(wide):
-        normed_out[:, i * step : (i + 1) * step] = (w * scale * gains[:, i * step : (i + 1) * step]).astype(bf16)
-    normed = normed_out[...]
-    copies[1].wait()
-    copies[2].wait()
-    made = dot(normed, both[...])
-    key, value = made[:, :half], made[:, half:]
+    return lambda at: copies[at].wait()
+
+
+def queries_kernel(tok, gain, wq, q_out, gained_out, scale_out, gains, held, sems):
+    wait = fetched((gain, wq), (gains, held), sems)
+    cores, chips, rows, step = tok.shape
+    total = jnp.zeros((rows, step), f32)
+    wait(0)
+    for x in range(chips):
+        for c in range(cores):
+            w = tok[c, x].astype(f32)
+            total = total + w * w
+            cols = slice((x * cores + c) * step, (x * cores + c + 1) * step)
+            gained_out[:, cols] = (w * gains[:, cols]).astype(bf16)
+    wait(1)
+    mean = jnp.sum(total, axis=1, keepdims=True) / (chips * cores * step)
+    scale = jnp.broadcast_to(lax.rsqrt(mean + epsilon), (rows, TILE))
+    scale_out[...] = scale
+    query = (dot(gained_out[...], held[...]) * scale).astype(bf16)
+    turned = jnp.transpose(query.astype(f32)).astype(bf16)
+    for i in range(q_out.shape[0]):
+        q_out[i, 0] = turned[:HEAD_DIM]
+        q_out[i, 1] = turned[HEAD_DIM:]
+
+
+def rest_kernel(gained_in, scale_in, wk, wv, wqw, wkw, wvw, kv_out, qw_out, kvw_out, both, held, narrow, sems):
+    half = wk.shape[1]
+    wait = fetched(
+        (wk, wv, wqw, wkw, wvw),
+        (both.at[:, :half], both.at[:, half:], held, narrow.at[:HEAD_DIM], narrow.at[HEAD_DIM:]),
+        sems,
+    )
+    gained = gained_in[...]
+    scale = scale_in[...]
+    wait(3)
+    wait(4)
+    kvw_out[...] = (dot(gained, narrow[...], 1, 1) * scale).astype(bf16)
+    wait(0)
+    wait(1)
+    made = dot(gained, both[...])
+    key, value = made[:, :half] * scale, made[:, half:] * scale
     first = lax.broadcasted_iota(jnp.int32, (TILE, TILE), 1) < HEAD_DIM
     heads = [
         jnp.where(first, key, pltpu.roll(value, HEAD_DIM, 1)).astype(bf16),
@@ -112,19 +113,8 @@
     ]
     for i in range(kv_out.shape[0]):
         kv_out[i] = heads[i % 2]
-
-
-def rest_kernel(normed_in, wq, wqw, wkw, wvw, q_out, qw_out, kvw_out, *held):
-    ready = fetched((wkw, wvw, wq, wqw), held[:4], held[4])
-    normed = normed_in[...]
-    kvw_out[:, :HEAD_DIM] = dot(normed, ready(0), 1, 1).astype(bf16)
-    kvw_out[:, HEAD_DIM:] = dot(normed, ready(1), 1, 1).astype(bf16)
-    query = dot(normed, ready(2)).astype(bf16)
-    turned = jnp.transpose(query.astype(f32)).astype(bf16)
-    for i in range(q_out.shape[0]):
-        q_out[i, 0] = turned[:HEAD_DIM]
-        q_out[i, 1] = turned[HEAD_DIM:]
-    qw_out[...] = dot(normed, ready(3)).astype(bf16)
+    wait(2)
+    qw_out[...] = (dot(gained, held[...]) * scale).astype(bf16)
 
 
 def stick_kernel(bias, q, kv, out, weight, keys, values):
@@ -309,41 +299,42 @@
     def swap(value, axis):
         return lax.all_to_all(value, axis, 0, 0, tiled=True)
 
-    gathered = lax.all_gather(tokens, TP, axis=0, tiled=True).reshape(ntp, tok_rows, feats)
+    chips = lax.axis_size("x")
+    from_chips = lax.all_to_all(jnp.broadcast_to(tokens[None], (chips, tok_rows, feats)), "x", 0, 0, tiled=True)
+    gathered = lax.all_gather(from_chips, "core")
     head_pair = w_key_stick.shape[1]
 
-    def holders(arrays):
-        return [pltpu.VMEM(a.shape, a.dtype) for a in arrays] + [pltpu.SemaphoreType.DMA((PIECES * len(arrays),))]
-
-    gain = pre_gain.reshape(1, width)
-    kv_all, normed = call(
-        keys_kernel,
+    wide = jax.ShapeDtypeStruct((tok_rows, width), bf16)
+    block = jax.ShapeDtypeStruct((tok_rows, head_pair), bf16)
+    q_all, gained, scale = call(
+        queries_kernel,
         (
-            jax.ShapeDtypeStruct((ROWS, tok_rows, head_pair), bf16),
-            jax.ShapeDtypeStruct((tok_rows, width), bf16),
+            jax.ShapeDtypeStruct((nz, 2, HEAD_DIM, tok_rows), bf16),
+            wide,
+            jax.ShapeDtypeStruct((tok_rows, TILE), f32),
         ),
-        [VM, HB, HB, HB],
+        [VM, HB, HB],
+        scratch=[
+            pltpu.VMEM((1, width), f32),
+            pltpu.VMEM(w_query_stick.shape, bf16),
+            pltpu.SemaphoreType.DMA((2,)),
+        ],
+    )(gathered, pre_gain.reshape(1, width), w_query_stick)
+    q_col = swap(q_all.reshape(2 * nz, HEAD_DIM, tok_rows), ("z", "hy"))
+    kv_all, q_win, kv_win = call(
+        rest_kernel,
+        (jax.ShapeDtypeStruct((ROWS, tok_rows, head_pair), bf16), block, block),
+        [VM] * 2 + [HB] * 5,
         scratch=[
             pltpu.VMEM((width, 2 * head_pair), bf16),
-            pltpu.VMEM((1, width), f32),
-            pltpu.SemaphoreType.DMA((3,)),
+            pltpu.VMEM(w_query_window.shape, bf16),
+            pltpu.VMEM((2 * HEAD_DIM, width), bf16),
+            pltpu.SemaphoreType.DMA((5,)),
         ],
-    )(gathered, gain, w_key_stick, w_value_stick)
-    kv_row = swap(kv_all, ("yy", "hy"))
-    weights = (w_query_stick, w_query_window, w_key_window.T, w_value_window.T)
-    q_all, q_win, kv_win = call(
-        rest_kernel,
-        (
-            jax.ShapeDtypeStruct((nz, 2, HEAD_DIM, tok_rows), bf16),
-            jax.ShapeDtypeStruct((tok_rows, head_pair), bf16),
-            jax.ShapeDtypeStruct((tok_rows, head_pair), bf16),
-        ),
-        [VM] + [HB] * 4,
-        scratch=holders((weights[2], weights[3], weights[0], weights[1])),
-    )(normed, *weights)
+    )(gained, scale, w_key_stick, w_value_stick, w_query_window, w_key_window.T, w_value_window.T)
     count = nz * ROWS
     previous = lax.ppermute(kv_win, ("z", "yy", "hy"), [(i, i + 1) for i in range(count - 1)])
-    q_col = swap(q_all.reshape(2 * nz, HEAD_DIM, tok_rows), ("z", "hy"))
+    kv_row = swap(kv_all, ("yy", "hy"))
     rows = tok_rows // ntp
     halves = (jax.ShapeDtypeStruct((ntp // 2, rows, width + TILE), bf16),) * 2
     keep_w, send_w = call(window_kernel, halves, [SM] + [VM] * 5)(

time: 99.2 us -> 98.4 us (level)
  the two profiles are of different devices: /device:TPU:1 before, /device:TPU:64 now
where the time goes in v5:
time: 98.4 us; the launch traced here: 97.9 us
  blocking collectives  63 us (64%)
  Pallas kernels  14.2 us (14%)
  starting transfers between devices  13.1 us (13%)
  waiting for transfers between devices  5.91 us (6%)
  local copies, waits for them, and re-layouts  1.55 us (2%)
    all_to_all x3, blocking collectives, swap(): return lax.all_to_all(value, axis, 0, 0, tiled=True)  50.1 us
    pallas_call x7, Pallas kernels, begun(): run(*[pltpu.with_memory_space_constraint(a, spaces[id(spec)]) if id(spec)...  14.2 us
    all_to_all x1, blocking collectives, shards(): lax.all_to_all(jnp.broadcast_to(tokens[None], (chips, tok_rows, feats)),...  10.8 us
    all_to_all x1, starting transfers between devices, swap(): return lax.all_to_all(value, axis, 0, 0, tiled=True)  5.4 us
    ppermute x1, waiting for transfers between devices, shards(): lax.ppermute(kv_win, ('z', 'yy', 'hy'), [(i, i + 1) for i in range(count...  4.76 us
    ppermute x2, starting transfers between devices, to_other_core(): return lax.ppermute(value, 'core', [(0, 1), (1, 0)])  4.32 us
    ppermute x1, starting transfers between devices, shards(): lax.ppermute(kv_win, ('z', 'yy', 'hy'), [(i, i + 1) for i in range(count...  3.37 us
    all_gather x1, blocking collectives, shards(): gathered = lax.all_gather(from_chips, 'core')  2.17 us
  transfers between devices with their start and end apart: 4, of which 2 were waited for; matrix products, arithmetic and copies ran while one was open for 0% of the time, Pallas kernels for 2%

profile of v5, /device:TPU:64, one launch (start us, length us, event | category | flops | bytes accessed | tf_op | source)
XLA Modules:
  0.0 97.9 jit_solution(7590476890377078787)
XLA Ops:
  0.0 0.9 broadcast_in_dim.2
  0.9 10.8 %all_to_all.25 = bf16[4,128,256]{2,1,0:T(8,128)(2,1)S(1)} all-to-all(bf16[4,128,256]{2,1,0:T(8,128)(2,1)S(1)} %broadcast_in_dim.2), channel_id=1, replica_groups=mesh['z'=8,'yy'=4,'hy'=2,'x'=4,'core'=2] {'x'}, dimensions={0} | all-to-all | bytes 524288 | tf_op jit(solution)/shard_map/all_to_all | solution.py:303
  11.6 2.2 %all-gather = bf16[8,128,256]{2,1,0:T(8,128)(2,1)S(1)} all-gather(bf16[4,128,256]{2,1,0:T(8,128)(2,1)S(1)} %all_to_all.25), channel_id=2, replica_groups=mesh['z'=8,'yy'=4,'hy'=2,'x'=4,'core'=2] {'core'}, dimensions={0}, use_global_device_ids=true | all-gather | bytes 786432 | tf_op jit(solution)/shard_map/all_gather | solution.py:304
  13.8 1.4 %shard_map.145 = (bf16[8,2,64,128]{3,2,1,0:T(8,128)(2,1)S(1)}, bf16[128,2048]{1,0:T(8,128)(2,1)S(1)}, f32[128,128]{1,0:T(8,128)S(1)}) custom-call(bf16[2,4,128,256]{3,2,1,0:T(8,128)(2,1)S(1)} %bitcast.8, f32[1,2048]{1,0:T(1,128)} %bitcast.15, bf16[2048,128]{1,0:T(8,128)(2,1)} %wq.1), custom_call_target="tpu_custom_call" | custom-call | tf_op jit(solution)/shard_map/pallas_call | solution.py:45
  15.2 2.8 %shard_map.146 = (bf16[8,128,128]{2,1,0:T(8,128)(2,1)S(1)}, bf16[128,128]{1,0:T(8,128)(2,1)S(1)}, bf16[128,128]{1,0:T(8,128)(2,1)S(1)}) custom-call(bf16[128,2048]{1,0:T(8,128)(2,1)S(1)} %get-tuple-element.16.gained_in, f32[128,128]{1,0:T(8,128)S(1)} %get-tuple-element.17.scale_in, bf16[2048,128]{1,0:T(8,128)(2,1)} %wk.1, bf16[2048,128]{1,0:T(8,128)(2,1)} %wv.1, ...), custom_call_target="tpu_custom_call" | custom-call | tf_op jit(solution)/shard_map/pallas_call | solution.py:45
  18.0 19.1 %all_to_all.26.kv = bf16[8,128,128]{2,1,0:T(8,128)(2,1)S(1)} all-to-all(bf16[8,128,128]{2,1,0:T(8,128)(2,1)S(1)} %get-tuple-element.18), channel_id=1, replica_groups=mesh['z'=8,'yy'=4,'hy'=2,'x'=4,'core'=2] {'yy','hy'}, dimensions={0} | all-to-all | bytes 524288 | tf_op jit(solution)/shard_map/all_to_all | solution.py:300
  37.1 0.0 copy-start.5
  37.1 18.1 %all_to_all.27.q = bf16[16,64,128]{2,1,0:T(8,128)(2,1)S(1)} all-to-all(bf16[16,64,128]{2,1,0:T(8,128)(2,1)S(1)} %bitcast.9), channel_id=1, replica_groups=mesh['z'=8,'yy'=4,'hy'=2,'x'=4,'core'=2] {'z','hy'}, dimensions={0} | all-to-all | bytes 524288 | tf_op jit(solution)/shard_map/all_to_all | solution.py:300
  55.2 0.0 copy-done.5
  55.2 0.0 copy-start
  55.2 7.1 %shard_map.147 = bf16[16,72,128]{2,1,0:T(8,128)(2,1)} custom-call(f32[2]{0:T(128)S(1)} %copy-done.5, bf16[16,64,128]{2,1,0:T(8,128)(2,1)S(1)} %all_to_all.27.q, bf16[8,128,128]{2,1,0:T(8,128)(2,1)S(1)} %all_to_all.26.kv), custom_call_target="tpu_custom_call" | custom-call | tf_op jit(solution)/shard_map/pallas_call | solution.py:45
  62.4 5.4 %all-to-all-start.3 = ((bf16[16,72,128]{2,1,0:T(8,128)(2,1)}), bf16[16,72,128]{2,1,0:T(8,128)(2,1)S(1)}, u32[]{:S(2)}, u32[]{:S(2)}) async-start(bf16[16,72,128]{2,1,0:T(8,128)(2,1)} %shard_map.147), calls=%async_computation.3 | async-start | bytes 589824 | tf_op jit(solution)/shard_map/all_to_all | solution.py:300
  67.8 3.4 %collective-permute-start.1 = (bf16[128,128]{1,0:T(8,128)(2,1)S(1)}, bf16[128,128]{1,0:T(8,128)(2,1)S(1)}, u32[]{:S(2)}, u32[]{:S(2)}) collective-permute-start(bf16[128,128]{1,0:T(8,128)(2,1)S(1)} %get-tuple-element.22.own), channel_id=1, source_target_pairs={{0,8},{8,16},{16,24},{24,32},{32,40},{40,48},{48,56},{56,64},{64,7... | collective-permute-start | bytes 98312 | tf_op jit(solution)/shard_map/ppermute | solution.py:336
  71.1 4.8 %collective-permute-done.1.prev = bf16[128,128]{1,0:T(8,128)(2,1)S(1)} collective-permute-done((bf16[128,128]{1,0:T(8,128)(2,1)S(1)}, bf16[128,128]{1,0:T(8,128)(2,1)S(1)}, u32[]{:S(2)}, u32[]{:S(2)}) %collective-permute-start.1) | collective-permute-done | bytes 32800 | tf_op jit(solution)/shard_map/ppermute | solution.py:336
  75.9 0.0 copy-done
  75.9 0.6 copy-done.3
  76.6 0.0 copy-done.4
  76.6 1.3 %shard_map.149 = (bf16[4,16,2176]{2,1,0:T(8,128)(2,1)S(1)}, bf16[4,16,2176]{2,1,0:T(8,128)(2,1)S(1)}) custom-call(f32[2]{0:T(128)S(1)} %copy-done.3, bf16[128,128]{1,0:T(8,128)(2,1)S(1)} %get-tuple-element.21.qw, bf16[128,128]{1,0:T(8,128)(2,1)S(1)} %collective-permute-done.1.prev, bf16[128,128]{1,0:T(8,128)(2,1)S(1)} %get-tuple-element.22.own, ...), custom_call_target="tpu_custom_call" | custom-call | tf_op jit(solution)/shard_map/pallas_call | solution.py:45
  77.9 0.0 copy-start.6
  77.9 1.9 %collective-permute-start.2 = (bf16[4,16,2176]{2,1,0:T(8,128)(2,1)S(1)}, bf16[4,16,2176]{2,1,0:T(8,128)(2,1)S(1)}, u32[]{:S(2)}, u32[]{:S(2)}) collective-permute-start(bf16[4,16,2176]{2,1,0:T(8,128)(2,1)S(1)} %get-tuple-element.24), channel_id=1, source_target_pairs={{0,1},{1,0},{2,3},{3,2},{4,5},{5,4},{6,7},{7,6},{8,9},{9,8},{10,11... | collective-permute-start | bytes 835592 | tf_op jit(solution)/shard_map/ppermute | solution.py:345
  79.8 0.0 all-to-all-done.3.parts
  79.8 0.0 copy-done.1
  79.9 0.0 copy-done.6
  79.9 0.4 shard_map.148
  80.3 2.4 %collective-permute-start = (bf16[4,16,2176]{2,1,0:T(8,128)(2,1)S(1)}, bf16[4,16,2176]{2,1,0:T(8,128)(2,1)S(1)}, u32[]{:S(2)}, u32[]{:S(2)}) collective-permute-start(bf16[4,16,2176]{2,1,0:T(8,128)(2,1)S(1)} %get-tuple-element.20), channel_id=1, source_target_pairs={{0,1},{1,0},{2,3},{3,2},{4,5},{5,4},{6,7},{7,6},{8,9},{9,8},{10,11... | collective-permute-start | bytes 835592 | tf_op jit(solution)/shard_map/ppermute | solution.py:345
  82.7 0.0 collective-permute-done.2.came_w
  82.7 1.2 %collective-permute-done.came_s = bf16[4,16,2176]{2,1,0:T(8,128)(2,1)S(1)} collective-permute-done((bf16[4,16,2176]{2,1,0:T(8,128)(2,1)S(1)}, bf16[4,16,2176]{2,1,0:T(8,128)(2,1)S(1)}, u32[]{:S(2)}, u32[]{:S(2)}) %collective-permute-start) | collective-permute-done | bytes 278560 | tf_op jit(solution)/shard_map/ppermute | solution.py:345
  83.8 0.3 shard_map.150
  84.1 0.0 copy-start.2
  84.1 12.8 %all_to_all.28.parts = bf16[4,16,4224]{2,1,0:T(8,128)(2,1)S(1)} all-to-all(bf16[4,16,4224]{2,1,0:T(8,128)(2,1)S(1)} %shard_map.150), channel_id=1, replica_groups=mesh['z'=8,'yy'=4,'hy'=2,'x'=4,'core'=2] {'x'}, dimensions={0} | all-to-all | bytes 1081344 | tf_op jit(solution)/shard_map/all_to_all | solution.py:300
  97.0 0.0 copy-done.2
  97.0 0.9 shard_map.151
  (3 shorter events, 0.0 us)
Async XLA Ops:
  37.1 18.1 %copy-start.5 = (f32[2]{0:T(128)S(1)}, f32[2]{0:T(128)}, u32[]{:S(2)}) copy-start(f32[2]{0:T(128)} %bias.1) | copy-start | bytes 28
  55.2 20.7 %copy-start = (bf16[128,2048]{1,0:T(8,128)(2,1)S(1)}, bf16[128,2048]{1,0:T(8,128)(2,1)}, u32[]{:S(2)}) copy-start(bf16[128,2048]{1,0:T(8,128)(2,1)} %w_out.3) | copy-start | bytes 1572868
  62.4 17.5 %copy-start.1 = (bf16[128,2048]{1,0:T(8,128)(2,1)S(1)}, bf16[128,2048]{1,0:T(8,128)(2,1)}, u32[]{:S(2)}) copy-start(bf16[128,2048]{1,0:T(8,128)(2,1)} %w_out.2) | copy-start | bytes 1572868
  62.4 17.5 %all-to-all-start.3 = ((bf16[16,72,128]{2,1,0:T(8,128)(2,1)}), bf16[16,72,128]{2,1,0:T(8,128)(2,1)S(1)}, u32[]{:S(2)}, u32[]{:S(2)}) async-start(bf16[16,72,128]{2,1,0:T(8,128)(2,1)} %shard_map.147), calls=%async_computation.3 | async-start | bytes 589824 | tf_op jit(solution)/shard_map/all_to_all | solution.py:300
  67.8 8.1 %collective-permute-start.1 = (bf16[128,128]{1,0:T(8,128)(2,1)S(1)}, bf16[128,128]{1,0:T(8,128)(2,1)S(1)}, u32[]{:S(2)}, u32[]{:S(2)}) collective-permute-start(bf16[128,128]{1,0:T(8,128)(2,1)S(1)} %get-tuple-element.22.own), channel_id=1, source_target_pairs={{0,8},{8,16},{16,24},{24,32},{32,40},{40,48},{48,56},{56,64},{64,7... | collective-permute-start | bytes 98312 | tf_op jit(solution)/shard_map/ppermute | solution.py:336
  75.9 0.7 copy-start.3
  75.9 0.7 copy-start.4
  77.9 2.0 %copy-start.6 = (f32[128]{0:T(128)S(1)}, f32[128]{0:T(128)}, u32[]{:S(2)}) copy-start(f32[128]{0:T(128)} %param.25) | copy-start | bytes 1540
  77.9 4.8 %collective-permute-start.2 = (bf16[4,16,2176]{2,1,0:T(8,128)(2,1)S(1)}, bf16[4,16,2176]{2,1,0:T(8,128)(2,1)S(1)}, u32[]{:S(2)}, u32[]{:S(2)}) collective-permute-start(bf16[4,16,2176]{2,1,0:T(8,128)(2,1)S(1)} %get-tuple-element.24), channel_id=1, source_target_pairs={{0,1},{1,0},{2,3},{3,2},{4,5},{5,4},{6,7},{7,6},{8,9},{9,8},{10,11... | collective-permute-start | bytes 835592 | tf_op jit(solution)/shard_map/ppermute | solution.py:345
  80.3 3.6 %collective-permute-start = (bf16[4,16,2176]{2,1,0:T(8,128)(2,1)S(1)}, bf16[4,16,2176]{2,1,0:T(8,128)(2,1)S(1)}, u32[]{:S(2)}, u32[]{:S(2)}) collective-permute-start(bf16[4,16,2176]{2,1,0:T(8,128)(2,1)S(1)} %get-tuple-element.20), channel_id=1, source_target_pairs={{0,1},{1,0},{2,3},{3,2},{4,5},{5,4},{6,7},{7,6},{8,9},{9,8},{10,11... | collective-permute-start | bytes 835592 | tf_op jit(solution)/shard_map/ppermute | solution.py:345
  84.1 12.9 %copy-start.2 = (f32[2048]{0:T(1024)S(1)}, f32[2048]{0:T(1024)}, u32[]{:S(2)}) copy-start(f32[2048]{0:T(1024)} %param.29) | copy-start | bytes 24580

commit v6 on v5

--- a/solution.py
+++ b/solution.py
@@ -68,44 +68,39 @@
     return lambda at: copies[at].wait()
 
 
-def queries_kernel(tok, gain, wq, q_out, gained_out, scale_out, gains, held, sems):
+def queries_kernel(tok, gain, wq, q_out, normed_out, gains, held, sems):
     wait = fetched((gain, wq), (gains, held), sems)
-    cores, chips, rows, step = tok.shape
-    total = jnp.zeros((rows, step), f32)
+    cores, chips, _, step = tok.shape
+    wide = [tok[c, x].astype(f32) for x in range(chips) for c in range(cores)]
+    total = sum(w * w for w in wide)
+    scale = lax.rsqrt(jnp.sum(total, axis=1, keepdims=True) / (len(wide) * step) + epsilon)
     wait(0)
-    for x in range(chips):
-        for c in range(cores):
-            w = tok[c, x].astype(f32)
-            total = total + w * w
-            cols = slice((x * cores + c) * step, (x * cores + c + 1) * step)
-            gained_out[:, cols] = (w * gains[:, cols]).astype(bf16)
+    for i, w in enumerate(wide):
+        cols = slice(i * step, (i + 1) * step)
+        normed_out[:, cols] = (w * scale * gains[:, cols]).astype(bf16)
     wait(1)
-    mean = jnp.sum(total, axis=1, keepdims=True) / (chips * cores * step)
-    scale = jnp.broadcast_to(lax.rsqrt(mean + epsilon), (rows, TILE))
-    scale_out[...] = scale
-    query = (dot(gained_out[...], held[...]) * scale).astype(bf16)
+    query = dot(normed_out[...], held[...]).astype(bf16)
     turned = jnp.transpose(query.astype(f32)).astype(bf16)
     for i in range(q_out.shape[0]):
         q_out[i, 0] = turned[:HEAD_DIM]
         q_out[i, 1] = turned[HEAD_DIM:]
 
 
-def rest_kernel(gained_in, scale_in, wk, wv, wqw, wkw, wvw, kv_out, qw_out, kvw_out, both, held, narrow, sems):
+def rest_kernel(normed_in, wk, wv, wqw, wkw, wvw, kv_out, qw_out, kvw_out, both, held, narrow, sems):
     half = wk.shape[1]
     wait = fetched(
         (wk, wv, wqw, wkw, wvw),
         (both.at[:, :half], both.at[:, half:], held, narrow.at[:HEAD_DIM], narrow.at[HEAD_DIM:]),
         sems,
     )
-    gained = gained_in[...]
-    scale = scale_in[...]
+    normed = normed_in[...]
     wait(3)
     wait(4)
-    kvw_out[...] = (dot(gained, narrow[...], 1, 1) * scale).astype(bf16)
+    kvw_out[...] = dot(normed, narrow[...], 1, 1).astype(bf16)
     wait(0)
     wait(1)
-    made = dot(gained, both[...])
-    key, value = made[:, :half] * scale, made[:, half:] * scale
+    made = dot(normed, both[...])
+    key, value = made[:, :half], made[:, half:]
     first = lax.broadcasted_iota(jnp.int32, (TILE, TILE), 1) < HEAD_DIM
     heads = [
         jnp.where(first, key, pltpu.roll(value, HEAD_DIM, 1)).astype(bf16),
@@ -114,7 +109,7 @@
     for i in range(kv_out.shape[0]):
         kv_out[i] = heads[i % 2]
     wait(2)
-    qw_out[...] = (dot(gained, held[...]) * scale).astype(bf16)
+    qw_out[...] = dot(normed, held[...]).astype(bf16)
 
 
 def stick_kernel(bias, q, kv, out, weight, keys, values):
@@ -189,7 +184,8 @@
     lax.fori_loop(0, lax.div(last - row, 2), later, 0)
 
 
-def window_kernel(sinks, qw, prev, own, w_out, gain, keep, send):
+def window_kernel(sinks, qw, prev, own, w_out, gain, stick_gain, keep, send, stick_gain_out):
+    stick_gain_out[...] = stick_gain[...]
     lane = lax.broadcasted_iota(jnp.int32, (TILE, TILE), 1)
     first = lane < HEAD_DIM
     block = lax.axis_index("z") + lax.axis_index("yy") + lax.axis_index("hy")
@@ -306,13 +302,9 @@
 
     wide = jax.ShapeDtypeStruct((tok_rows, width), bf16)
     block = jax.ShapeDtypeStruct((tok_rows, head_pair), bf16)
-    q_all, gained, scale = call(
+    q_all, normed = call(
         queries_kernel,
-        (
-            jax.ShapeDtypeStruct((nz, 2, HEAD_DIM, tok_rows), bf16),
-            wide,
-            jax.ShapeDtypeStruct((tok_rows, TILE), f32),
-        ),
+        (jax.ShapeDtypeStruct((nz, 2, HEAD_DIM, tok_rows), bf16), wide),
         [VM, HB, HB],
         scratch=[
             pltpu.VMEM((1, width), f32),
@@ -324,21 +316,22 @@
     kv_all, q_win, kv_win = call(
         rest_kernel,
         (jax.ShapeDtypeStruct((ROWS, tok_rows, head_pair), bf16), block, block),
-        [VM] * 2 + [HB] * 5,
+        [VM] + [HB] * 5,
         scratch=[
             pltpu.VMEM((width, 2 * head_pair), bf16),
             pltpu.VMEM(w_query_window.shape, bf16),
             pltpu.VMEM((2 * HEAD_DIM, width), bf16),
             pltpu.SemaphoreType.DMA((5,)),
         ],
-    )(gained, scale, w_key_stick, w_value_stick, w_query_window, w_key_window.T, w_value_window.T)
+    )(normed, w_key_stick, w_value_stick, w_query_window, w_key_window.T, w_value_window.T)
     count = nz * ROWS
     previous = lax.ppermute(kv_win, ("z", "yy", "hy"), [(i, i + 1) for i in range(count - 1)])
     kv_row = swap(kv_all, ("yy", "hy"))
     rows = tok_rows // ntp
     halves = (jax.ShapeDtypeStruct((ntp // 2, rows, width + TILE), bf16),) * 2
-    keep_w, send_w = call(window_kernel, halves, [SM] + [VM] * 5)(
-        sinks, q_win, previous, kv_win, w_out_window, window_gain.reshape(1, -1)
+    gain_row = jax.ShapeDtypeStruct((1, head_pair), f32)
+    keep_w, send_w, stick_gain = call(window_kernel, (*halves, gain_row), [SM] + [VM] * 6)(
+        sinks, q_win, previous, kv_win, w_out_window, window_gain.reshape(1, -1), stick_gain.reshape(1, -1)
     )
 
     def to_other_core(value):
@@ -356,7 +349,9 @@
         ],
     )(stick_bias, q_col, kv_row)
     returned = swap(partial, ("z", "hy"))
-    keep_s, send_s = call(combine_kernel, halves, [VM] * 3)(returned, stick_gain.reshape(1, -1), w_out_stick)
+    keep_s, send_s = call(combine_kernel, halves, [VM] * 3)(
+        returned, stick_gain, w_out_stick
+    )
     came_s = to_other_core(send_s)
     sending = call(
         pairs_kernel, jax.ShapeDtypeStruct((ntp // 2, rows, 2 * width + TILE), bf16), [VM] * 4

time: 98.4 us -> 98.5 us (level)
  no operation moved by 1% of the time
where the time goes in v6:
time: 98.5 us; the launch traced here: 98 us
  blocking collectives  63 us (64%)
  Pallas kernels  14.3 us (15%)
  starting transfers between devices  13.1 us (13%)
  waiting for transfers between devices  5.91 us (6%)
  local copies, waits for them, and re-layouts  1.55 us (2%)
    all_to_all x3, blocking collectives, swap(): return lax.all_to_all(value, axis, 0, 0, tiled=True)  50.1 us
    pallas_call x7, Pallas kernels, begun(): run(*[pltpu.with_memory_space_constraint(a, spaces[id(spec)]) if id(spec)...  14.3 us
    all_to_all x1, blocking collectives, shards(): lax.all_to_all(jnp.broadcast_to(tokens[None], (chips, tok_rows, feats)),...  10.8 us
    all_to_all x1, starting transfers between devices, swap(): return lax.all_to_all(value, axis, 0, 0, tiled=True)  5.42 us
    ppermute x1, waiting for transfers between devices, shards(): lax.ppermute(kv_win, ('z', 'yy', 'hy'), [(i, i + 1) for i in range(count...  4.76 us
    ppermute x2, starting transfers between devices, to_other_core(): return lax.ppermute(value, 'core', [(0, 1), (1, 0)])  4.33 us
    ppermute x1, starting transfers between devices, shards(): lax.ppermute(kv_win, ('z', 'yy', 'hy'), [(i, i + 1) for i in range(count...  3.37 us
    all_gather x1, blocking collectives, shards(): gathered = lax.all_gather(from_chips, 'core')  2.17 us
  transfers between devices with their start and end apart: 4, of which 2 were waited for; matrix products, arithmetic and copies ran while one was open for 0% of the time, Pallas kernels for 2%

profile of v6, /device:TPU:64, one launch (start us, length us, event | category | flops | bytes accessed | tf_op | source)
XLA Modules:
  0.0 98.0 jit_solution(14305578964798321266)
XLA Ops:
  0.0 0.9 broadcast_in_dim.2
  0.9 10.8 %all_to_all.25 = bf16[4,128,256]{2,1,0:T(8,128)(2,1)S(1)} all-to-all(bf16[4,128,256]{2,1,0:T(8,128)(2,1)S(1)} %broadcast_in_dim.2), channel_id=1, replica_groups=mesh['z'=8,'yy'=4,'hy'=2,'x'=4,'core'=2] {'x'}, dimensions={0} | all-to-all | bytes 524288 | tf_op jit(solution)/shard_map/all_to_all | solution.py:299
  11.6 2.2 %all-gather = bf16[8,128,256]{2,1,0:T(8,128)(2,1)S(1)} all-gather(bf16[4,128,256]{2,1,0:T(8,128)(2,1)S(1)} %all_to_all.25), channel_id=2, replica_groups=mesh['z'=8,'yy'=4,'hy'=2,'x'=4,'core'=2] {'core'}, dimensions={0}, use_global_device_ids=true | all-gather | bytes 786432 | tf_op jit(solution)/shard_map/all_gather | solution.py:300
  13.8 1.5 %shard_map.145 = (bf16[8,2,64,128]{3,2,1,0:T(8,128)(2,1)S(1)}, bf16[128,2048]{1,0:T(8,128)(2,1)S(1)}) custom-call(bf16[2,4,128,256]{3,2,1,0:T(8,128)(2,1)S(1)} %bitcast.8, f32[1,2048]{1,0:T(1,128)} %bitcast.15, bf16[2048,128]{1,0:T(8,128)(2,1)} %wq.1), custom_call_target="tpu_custom_call" | custom-call | tf_op jit(solution)/shard_map/pallas_call | solution.py:45
  15.3 2.8 %shard_map.146 = (bf16[8,128,128]{2,1,0:T(8,128)(2,1)S(1)}, bf16[128,128]{1,0:T(8,128)(2,1)S(1)}, bf16[128,128]{1,0:T(8,128)(2,1)S(1)}) custom-call(bf16[128,2048]{1,0:T(8,128)(2,1)S(1)} %get-tuple-element.16.normed_in, bf16[2048,128]{1,0:T(8,128)(2,1)} %wk.1, bf16[2048,128]{1,0:T(8,128)(2,1)} %wv.1, bf16[2048,128]{1,0:T(8,128)(2,1)} %wqw.1, ...), custom_call_target="tpu_custom_call" | custom-call | tf_op jit(solution)/shard_map/pallas_call | solution.py:45
  18.1 19.1 %all_to_all.26.kv = bf16[8,128,128]{2,1,0:T(8,128)(2,1)S(1)} all-to-all(bf16[8,128,128]{2,1,0:T(8,128)(2,1)S(1)} %get-tuple-element.17), channel_id=1, replica_groups=mesh['z'=8,'yy'=4,'hy'=2,'x'=4,'core'=2] {'yy','hy'}, dimensions={0} | all-to-all | bytes 524288 | tf_op jit(solution)/shard_map/all_to_all | solution.py:296
  37.2 0.0 copy-start.3
  37.2 18.2 %all_to_all.27.q = bf16[16,64,128]{2,1,0:T(8,128)(2,1)S(1)} all-to-all(bf16[16,64,128]{2,1,0:T(8,128)(2,1)S(1)} %bitcast.9), channel_id=1, replica_groups=mesh['z'=8,'yy'=4,'hy'=2,'x'=4,'core'=2] {'z','hy'}, dimensions={0} | all-to-all | bytes 524288 | tf_op jit(solution)/shard_map/all_to_all | solution.py:296
  55.3 0.0 copy-done.3
  55.3 0.0 copy-start
  55.3 7.1 %shard_map.147 = bf16[16,72,128]{2,1,0:T(8,128)(2,1)} custom-call(f32[2]{0:T(128)S(1)} %copy-done.3, bf16[16,64,128]{2,1,0:T(8,128)(2,1)S(1)} %all_to_all.27.q, bf16[8,128,128]{2,1,0:T(8,128)(2,1)S(1)} %all_to_all.26.kv), custom_call_target="tpu_custom_call" | custom-call | tf_op jit(solution)/shard_map/pallas_call | solution.py:45
  62.4 0.0 copy-start.1
  62.4 5.4 %all-to-all-start.3 = ((bf16[16,72,128]{2,1,0:T(8,128)(2,1)}), bf16[16,72,128]{2,1,0:T(8,128)(2,1)S(1)}, u32[]{:S(2)}, u32[]{:S(2)}) async-start(bf16[16,72,128]{2,1,0:T(8,128)(2,1)} %shard_map.147), calls=%async_computation.3 | async-start | bytes 589824 | tf_op jit(solution)/shard_map/all_to_all | solution.py:296
  67.9 3.4 %collective-permute-start = (bf16[128,128]{1,0:T(8,128)(2,1)S(1)}, bf16[128,128]{1,0:T(8,128)(2,1)S(1)}, u32[]{:S(2)}, u32[]{:S(2)}) collective-permute-start(bf16[128,128]{1,0:T(8,128)(2,1)S(1)} %get-tuple-element.19.own), channel_id=1, source_target_pairs={{0,8},{8,16},{16,24},{24,32},{32,40},{40,48},{48,56},{56,64},{64,7... | collective-permute-start | bytes 98312 | tf_op jit(solution)/shard_map/ppermute | solution.py:328
  71.2 4.8 %collective-permute-done.prev = bf16[128,128]{1,0:T(8,128)(2,1)S(1)} collective-permute-done((bf16[128,128]{1,0:T(8,128)(2,1)S(1)}, bf16[128,128]{1,0:T(8,128)(2,1)S(1)}, u32[]{:S(2)}, u32[]{:S(2)}) %collective-permute-start) | collective-permute-done | bytes 32800 | tf_op jit(solution)/shard_map/ppermute | solution.py:328
  76.0 0.0 copy-done
  76.0 0.6 copy-done.4
  76.7 0.0 copy-done.5
  76.7 0.0 copy-done.6
  76.7 1.3 %shard_map.148 = (bf16[4,16,2176]{2,1,0:T(8,128)(2,1)S(1)}, bf16[4,16,2176]{2,1,0:T(8,128)(2,1)S(1)}, f32[1,128]{1,0:T(1,128)S(1)}) custom-call(f32[2]{0:T(128)S(1)} %copy-done.4, bf16[128,128]{1,0:T(8,128)(2,1)S(1)} %get-tuple-element.18.qw, bf16[128,128]{1,0:T(8,128)(2,1)S(1)} %collective-permute-done.prev, bf16[128,128]{1,0:T(8,128)(2,1)S(1)} %get-tuple-element.19.own, ...), custom_call_target="tpu_custom_call" | custom-call | tf_op jit(solution)/shard_map/pallas_call | solution.py:45
  78.0 1.9 %collective-permute-start.2 = (bf16[4,16,2176]{2,1,0:T(8,128)(2,1)S(1)}, bf16[4,16,2176]{2,1,0:T(8,128)(2,1)S(1)}, u32[]{:S(2)}, u32[]{:S(2)}) collective-permute-start(bf16[4,16,2176]{2,1,0:T(8,128)(2,1)S(1)} %get-tuple-element.24), channel_id=1, source_target_pairs={{0,1},{1,0},{2,3},{3,2},{4,5},{5,4},{6,7},{7,6},{8,9},{9,8},{10,11... | collective-permute-start | bytes 835592 | tf_op jit(solution)/shard_map/ppermute | solution.py:338
  79.9 0.0 all-to-all-done.3.parts
  80.0 0.0 copy-done.1
  80.0 0.4 shard_map.149
  80.4 2.4 %collective-permute-start.1 = (bf16[4,16,2176]{2,1,0:T(8,128)(2,1)S(1)}, bf16[4,16,2176]{2,1,0:T(8,128)(2,1)S(1)}, u32[]{:S(2)}, u32[]{:S(2)}) collective-permute-start(bf16[4,16,2176]{2,1,0:T(8,128)(2,1)S(1)} %get-tuple-element.22), channel_id=1, source_target_pairs={{0,1},{1,0},{2,3},{3,2},{4,5},{5,4},{6,7},{7,6},{8,9},{9,8},{10,11... | collective-permute-start | bytes 835592 | tf_op jit(solution)/shard_map/ppermute | solution.py:338
  82.8 0.0 collective-permute-done.2.came_w
  82.8 1.2 %collective-permute-done.1.came_s = bf16[4,16,2176]{2,1,0:T(8,128)(2,1)S(1)} collective-permute-done((bf16[4,16,2176]{2,1,0:T(8,128)(2,1)S(1)}, bf16[4,16,2176]{2,1,0:T(8,128)(2,1)S(1)}, u32[]{:S(2)}, u32[]{:S(2)}) %collective-permute-start.1) | collective-permute-done | bytes 278560 | tf_op jit(solution)/shard_map/ppermute | solution.py:338
  83.9 0.3 shard_map.150
  84.2 0.0 copy-start.2
  84.2 12.8 %all_to_all.28.parts = bf16[4,16,4224]{2,1,0:T(8,128)(2,1)S(1)} all-to-all(bf16[4,16,4224]{2,1,0:T(8,128)(2,1)S(1)} %shard_map.150), channel_id=1, replica_groups=mesh['z'=8,'yy'=4,'hy'=2,'x'=4,'core'=2] {'x'}, dimensions={0} | all-to-all | bytes 1081344 | tf_op jit(solution)/shard_map/all_to_all | solution.py:296
  97.1 0.0 copy-done.2
  97.1 0.9 shard_map.151
  (3 shorter events, 0.0 us)
Async XLA Ops:
  37.2 18.2 %copy-start.3 = (f32[2]{0:T(128)S(1)}, f32[2]{0:T(128)}, u32[]{:S(2)}) copy-start(f32[2]{0:T(128)} %bias.1) | copy-start | bytes 28
  55.3 20.7 %copy-start = (bf16[128,2048]{1,0:T(8,128)(2,1)S(1)}, bf16[128,2048]{1,0:T(8,128)(2,1)}, u32[]{:S(2)}) copy-start(bf16[128,2048]{1,0:T(8,128)(2,1)} %w_out.2) | copy-start | bytes 1572868
  62.4 17.5 %copy-start.1 = (bf16[128,2048]{1,0:T(8,128)(2,1)S(1)}, bf16[128,2048]{1,0:T(8,128)(2,1)}, u32[]{:S(2)}) copy-start(bf16[128,2048]{1,0:T(8,128)(2,1)} %w_out.3) | copy-start | bytes 1572868
  62.4 17.5 %all-to-all-start.3 = ((bf16[16,72,128]{2,1,0:T(8,128)(2,1)}), bf16[16,72,128]{2,1,0:T(8,128)(2,1)S(1)}, u32[]{:S(2)}, u32[]{:S(2)}) async-start(bf16[16,72,128]{2,1,0:T(8,128)(2,1)} %shard_map.147), calls=%async_computation.3 | async-start | bytes 589824 | tf_op jit(solution)/shard_map/all_to_all | solution.py:296
  67.9 8.1 %collective-permute-start = (bf16[128,128]{1,0:T(8,128)(2,1)S(1)}, bf16[128,128]{1,0:T(8,128)(2,1)S(1)}, u32[]{:S(2)}, u32[]{:S(2)}) collective-permute-start(bf16[128,128]{1,0:T(8,128)(2,1)S(1)} %get-tuple-element.19.own), channel_id=1, source_target_pairs={{0,8},{8,16},{16,24},{24,32},{32,40},{40,48},{48,56},{56,64},{64,7... | collective-permute-start | bytes 98312 | tf_op jit(solution)/shard_map/ppermute | solution.py:328
  76.0 0.7 copy-start.4
  76.0 0.7 copy-start.5
  76.0 0.7 copy-start.6
  78.0 4.8 %collective-permute-start.2 = (bf16[4,16,2176]{2,1,0:T(8,128)(2,1)S(1)}, bf16[4,16,2176]{2,1,0:T(8,128)(2,1)S(1)}, u32[]{:S(2)}, u32[]{:S(2)}) collective-permute-start(bf16[4,16,2176]{2,1,0:T(8,128)(2,1)S(1)} %get-tuple-element.24), channel_id=1, source_target_pairs={{0,1},{1,0},{2,3},{3,2},{4,5},{5,4},{6,7},{7,6},{8,9},{9,8},{10,11... | collective-permute-start | bytes 835592 | tf_op jit(solution)/shard_map/ppermute | solution.py:338
  80.4 3.6 %collective-permute-start.1 = (bf16[4,16,2176]{2,1,0:T(8,128)(2,1)S(1)}, bf16[4,16,2176]{2,1,0:T(8,128)(2,1)S(1)}, u32[]{:S(2)}, u32[]{:S(2)}) collective-permute-start(bf16[4,16,2176]{2,1,0:T(8,128)(2,1)S(1)} %get-tuple-element.22), channel_id=1, source_target_pairs={{0,1},{1,0},{2,3},{3,2},{4,5},{5,4},{6,7},{7,6},{8,9},{9,8},{10,11... | collective-permute-start | bytes 835592 | tf_op jit(solution)/shard_map/ppermute | solution.py:338
  84.2 12.9 %copy-start.2 = (f32[2048]{0:T(1024)S(1)}, f32[2048]{0:T(1024)}, u32[]{:S(2)}) copy-start(f32[2048]{0:T(1024)} %param.29) | copy-start | bytes 24580

commit v7 on v6

--- a/solution.py
+++ b/solution.py
@@ -68,17 +68,21 @@
     return lambda at: copies[at].wait()
 
 
-def queries_kernel(tok, gain, wq, q_out, normed_out, gains, held, sems):
-    wait = fetched((gain, wq), (gains, held), sems)
+def spread_kernel(tok, gain, wq, tok_out, gain_out, wq_out, sems):
+    copies = [tok_out.at[i] for i in range(tok_out.shape[0])]
+    wait = fetched((tok,) * len(copies) + (gain, wq), (*copies, gain_out, wq_out), sems)
+    for i in range(len(copies) + 2):
+        wait(i)
+
+
+def queries_kernel(tok, gains, held, q_out, normed_out):
     cores, chips, _, step = tok.shape
     wide = [tok[c, x].astype(f32) for x in range(chips) for c in range(cores)]
     total = sum(w * w for w in wide)
     scale = lax.rsqrt(jnp.sum(total, axis=1, keepdims=True) / (len(wide) * step) + epsilon)
-    wait(0)
     for i, w in enumerate(wide):
         cols = slice(i * step, (i + 1) * step)
         normed_out[:, cols] = (w * scale * gains[:, cols]).astype(bf16)
-    wait(1)
     query = dot(normed_out[...], held[...]).astype(bf16)
     turned = jnp.transpose(query.astype(f32)).astype(bf16)
     for i in range(q_out.shape[0]):
@@ -246,10 +250,11 @@
 def pairs_kernel(keep_s, came_s, keep_w, came_w, out):
     width = keep_s.shape[2] - TILE
     lane = lax.broadcasted_iota(jnp.int32, (keep_s.shape[1], TILE), 1)
+    other = 1 - lax.axis_index("core")
     for at in range(out.shape[0]):
         parts = []
-        for n, (keep, came) in enumerate(((keep_s, came_s), (keep_w, came_w))):
-            both = keep[at].astype(f32) + came[at].astype(f32)
+        for n, (keep, came) in enumerate(((keep_s[at], came_s[other, at]), (keep_w[at], came_w[at]))):
+            both = keep.astype(f32) + came.astype(f32)
             out[at, :, n * width : (n + 1) * width] = both[:, :width].astype(bf16)
             parts += split(both[:, width : width + 1] + both[:, width + 1 : width + 2])
         tail = parts[-1].astype(f32)
@@ -296,22 +301,25 @@
         return lax.all_to_all(value, axis, 0, 0, tiled=True)
 
     chips = lax.axis_size("x")
-    from_chips = lax.all_to_all(jnp.broadcast_to(tokens[None], (chips, tok_rows, feats)), "x", 0, 0, tiled=True)
+    copies, gain, w_query = call(
+        spread_kernel,
+        (
+            jax.ShapeDtypeStruct((chips, tok_rows, feats), bf16),
+            jax.ShapeDtypeStruct((1, width), f32),
+            jax.ShapeDtypeStruct(w_query_stick.shape, bf16),
+        ),
+        [HB] * 3,
+        scratch=[pltpu.SemaphoreType.DMA((chips + 2,))],
+    )(tokens, pre_gain.reshape(1, width), w_query_stick)
+    from_chips = lax.all_to_all(copies, "x", 0, 0, tiled=True)
     gathered = lax.all_gather(from_chips, "core")
     head_pair = w_key_stick.shape[1]
 
     wide = jax.ShapeDtypeStruct((tok_rows, width), bf16)
     block = jax.ShapeDtypeStruct((tok_rows, head_pair), bf16)
     q_all, normed = call(
-        queries_kernel,
-        (jax.ShapeDtypeStruct((nz, 2, HEAD_DIM, tok_rows), bf16), wide),
-        [VM, HB, HB],
-        scratch=[
-            pltpu.VMEM((1, width), f32),
-            pltpu.VMEM(w_query_stick.shape, bf16),
-            pltpu.SemaphoreType.DMA((2,)),
-        ],
-    )(gathered, pre_gain.reshape(1, width), w_query_stick)
+        queries_kernel, (jax.ShapeDtypeStruct((nz, 2, HEAD_DIM, tok_rows), bf16), wide), [VM] * 3
+    )(gathered, gain, w_query)
     q_col = swap(q_all.reshape(2 * nz, HEAD_DIM, tok_rows), ("z", "hy"))
     kv_all, q_win, kv_win = call(
         rest_kernel,
@@ -352,7 +360,7 @@
     keep_s, send_s = call(combine_kernel, halves, [VM] * 3)(
         returned, stick_gain, w_out_stick
     )
-    came_s = to_other_core(send_s)
+    came_s = lax.all_gather(send_s, "core")
     sending = call(
         pairs_kernel, jax.ShapeDtypeStruct((ntp // 2, rows, 2 * width + TILE), bf16), [VM] * 4
     )(keep_s, came_s, keep_w, came_w)

time: 98.5 us -> 96.6 us (0.981)
  starting transfers between devices: 13.1 us -> 10.7 us
  blocking collectives: 63 us -> 65.3 us
  waiting for transfers between devices: 5.91 us -> 4.76 us
    ppermute x2 -> x1, starting transfers between devices: 4.33 us -> 1.92 us  [to_other_core(): return lax.ppermute(value, 'core', [(0, 1), (1, 0)])]
    all_gather x0 -> x1, blocking collectives: none -> 2.33 us  [shards(): came_s = lax.all_gather(send_s, 'core')]
    ppermute x2 -> x1, waiting for transfers between devices: 1.16 us -> 0.01 us  [to_other_core(): return lax.ppermute(value, 'core', [(0, 1), (1, 0)])]
    pallas_call x7 -> x8, Pallas kernels: 14.3 us -> 14.5 us  [begun(): run(*[pltpu.with_memory_space_constraint(a, spaces[id(spec)]) if id(spec)...]
  transfers between devices with their start and end apart: 4 -> 3, of which waited for: 2 -> 1; matrix products, arithmetic and copies ran while one was open for 0% -> 0% of each run, Pallas kernels for 2% -> 2%
where the time goes in v7:
time: 96.6 us; the launch traced here: 96.1 us
  blocking collectives  65.3 us (68%)
  Pallas kernels  14.5 us (15%)
  starting transfers between devices  10.7 us (11%)
  waiting for transfers between devices  4.76 us (5%)
    all_to_all x3, blocking collectives, swap(): return lax.all_to_all(value, axis, 0, 0, tiled=True)  50.1 us
    pallas_call x8, Pallas kernels, begun(): run(*[pltpu.with_memory_space_constraint(a, spaces[id(spec)]) if id(spec)...  14.5 us
    all_to_all x1, blocking collectives, shards(): from_chips = lax.all_to_all(copies, 'x', 0, 0, tiled=True)  10.8 us
    all_to_all x1, starting transfers between devices, swap(): return lax.all_to_all(value, axis, 0, 0, tiled=True)  5.42 us
    ppermute x1, waiting for transfers between devices, shards(): lax.ppermute(kv_win, ('z', 'yy', 'hy'), [(i, i + 1) for i in range(count...  4.76 us
    ppermute x1, starting transfers between devices, shards(): lax.ppermute(kv_win, ('z', 'yy', 'hy'), [(i, i + 1) for i in range(count...  3.37 us
    all_gather x1, blocking collectives, shards(): came_s = lax.all_gather(send_s, 'core')  2.33 us
    all_gather x1, blocking collectives, shards(): gathered = lax.all_gather(from_chips, 'core')  2.17 us
  transfers between devices with their start and end apart: 3, of which 1 were waited for; matrix products, arithmetic and copies ran while one was open for 0% of the time, Pallas kernels for 2%

profile of v7, /device:TPU:64, one launch (start us, length us, event | category | flops | bytes accessed | tf_op | source)
XLA Modules:
  0.0 96.1 jit_solution(12507666135882170949)
XLA Ops:
  0.0 1.2 %shard_map.145 = (bf16[4,128,256]{2,1,0:T(8,128)(2,1)S(1)}, f32[1,2048]{1,0:T(1,128)S(1)}, bf16[2048,128]{1,0:T(8,128)(2,1)S(1)}) custom-call(bf16[128,256]{1,0:T(8,128)(2,1)} %tok.1, f32[1,2048]{1,0:T(1,128)} %bitcast.17, bf16[2048,128]{1,0:T(8,128)(2,1)} %wq.1), custom_call_target="tpu_custom_call" | custom-call | tf_op jit(solution)/shard_map/pallas_call | solution.py:45
  1.3 10.8 %all_to_all.25 = bf16[4,128,256]{2,1,0:T(8,128)(2,1)S(1)} all-to-all(bf16[4,128,256]{2,1,0:T(8,128)(2,1)S(1)} %get-tuple-element.18), channel_id=1, replica_groups=mesh['z'=8,'yy'=4,'hy'=2,'x'=4,'core'=2] {'x'}, dimensions={0} | all-to-all | bytes 524288 | tf_op jit(solution)/shard_map/all_to_all | solution.py:314
  12.0 2.2 %all-gather = bf16[8,128,256]{2,1,0:T(8,128)(2,1)S(1)} all-gather(bf16[4,128,256]{2,1,0:T(8,128)(2,1)S(1)} %all_to_all.25), channel_id=2, replica_groups=mesh['z'=8,'yy'=4,'hy'=2,'x'=4,'core'=2] {'core'}, dimensions={0}, use_global_device_ids=true | all-gather | bytes 786432 | tf_op jit(solution)/shard_map/all_gather | solution.py:315
  14.2 0.5 shard_map.146
  14.7 2.8 %shard_map.147 = (bf16[8,128,128]{2,1,0:T(8,128)(2,1)S(1)}, bf16[128,128]{1,0:T(8,128)(2,1)S(1)}, bf16[128,128]{1,0:T(8,128)(2,1)S(1)}) custom-call(bf16[128,2048]{1,0:T(8,128)(2,1)S(1)} %get-tuple-element.22.normed_in, bf16[2048,128]{1,0:T(8,128)(2,1)} %wk.1, bf16[2048,128]{1,0:T(8,128)(2,1)} %wv.1, bf16[2048,128]{1,0:T(8,128)(2,1)} %wqw.1, ...), custom_call_target="tpu_custom_call" | custom-call | tf_op jit(solution)/shard_map/pallas_call | solution.py:45
  17.5 19.1 %all_to_all.26.kv = bf16[8,128,128]{2,1,0:T(8,128)(2,1)S(1)} all-to-all(bf16[8,128,128]{2,1,0:T(8,128)(2,1)S(1)} %get-tuple-element.23), channel_id=1, replica_groups=mesh['z'=8,'yy'=4,'hy'=2,'x'=4,'core'=2] {'yy','hy'}, dimensions={0} | all-to-all | bytes 524288 | tf_op jit(solution)/shard_map/all_to_all | solution.py:301
  36.6 0.0 copy-start.3
  36.6 18.2 %all_to_all.27.q = bf16[16,64,128]{2,1,0:T(8,128)(2,1)S(1)} all-to-all(bf16[16,64,128]{2,1,0:T(8,128)(2,1)S(1)} %bitcast.11), channel_id=1, replica_groups=mesh['z'=8,'yy'=4,'hy'=2,'x'=4,'core'=2] {'z','hy'}, dimensions={0} | all-to-all | bytes 524288 | tf_op jit(solution)/shard_map/all_to_all | solution.py:301
  54.7 0.0 copy-done.3
  54.7 0.0 copy-start
  54.7 7.1 %shard_map.148 = bf16[16,72,128]{2,1,0:T(8,128)(2,1)} custom-call(f32[2]{0:T(128)S(1)} %copy-done.3, bf16[16,64,128]{2,1,0:T(8,128)(2,1)S(1)} %all_to_all.27.q, bf16[8,128,128]{2,1,0:T(8,128)(2,1)S(1)} %all_to_all.26.kv), custom_call_target="tpu_custom_call" | custom-call | tf_op jit(solution)/shard_map/pallas_call | solution.py:45
  61.9 0.0 copy-start.1
  61.9 5.4 %all-to-all-start.3 = ((bf16[16,72,128]{2,1,0:T(8,128)(2,1)}), bf16[16,72,128]{2,1,0:T(8,128)(2,1)S(1)}, u32[]{:S(2)}, u32[]{:S(2)}) async-start(bf16[16,72,128]{2,1,0:T(8,128)(2,1)} %shard_map.148), calls=%async_computation.3 | async-start | bytes 589824 | tf_op jit(solution)/shard_map/all_to_all | solution.py:301
  67.3 3.4 %collective-permute-start = (bf16[128,128]{1,0:T(8,128)(2,1)S(1)}, bf16[128,128]{1,0:T(8,128)(2,1)S(1)}, u32[]{:S(2)}, u32[]{:S(2)}) collective-permute-start(bf16[128,128]{1,0:T(8,128)(2,1)S(1)} %get-tuple-element.25.own), channel_id=1, source_target_pairs={{0,8},{8,16},{16,24},{24,32},{32,40},{40,48},{48,56},{56,64},{64,7... | collective-permute-start | bytes 98312 | tf_op jit(solution)/shard_map/ppermute | solution.py:336
  70.7 4.8 %collective-permute-done.prev = bf16[128,128]{1,0:T(8,128)(2,1)S(1)} collective-permute-done((bf16[128,128]{1,0:T(8,128)(2,1)S(1)}, bf16[128,128]{1,0:T(8,128)(2,1)S(1)}, u32[]{:S(2)}, u32[]{:S(2)}) %collective-permute-start) | collective-permute-done | bytes 32800 | tf_op jit(solution)/shard_map/ppermute | solution.py:336
  75.4 0.0 copy-start.4
  75.4 0.0 copy-done
  75.4 0.6 copy-done.4
  76.1 0.0 copy-done.5
  76.1 0.0 copy-done.6
  76.1 1.3 %shard_map.149 = (bf16[4,16,2176]{2,1,0:T(8,128)(2,1)S(1)}, bf16[4,16,2176]{2,1,0:T(8,128)(2,1)S(1)}, f32[1,128]{1,0:T(1,128)S(1)}) custom-call(f32[2]{0:T(128)S(1)} %copy-done.4, bf16[128,128]{1,0:T(8,128)(2,1)S(1)} %get-tuple-element.24.qw, bf16[128,128]{1,0:T(8,128)(2,1)S(1)} %collective-permute-done.prev, bf16[128,128]{1,0:T(8,128)(2,1)S(1)} %get-tuple-element.25.own, ...), custom_call_target="tpu_custom_call" | custom-call | tf_op jit(solution)/shard_map/pallas_call | solution.py:45
  77.4 1.9 %collective-permute-start.1 = (bf16[4,16,2176]{2,1,0:T(8,128)(2,1)S(1)}, bf16[4,16,2176]{2,1,0:T(8,128)(2,1)S(1)}, u32[]{:S(2)}, u32[]{:S(2)}) collective-permute-start(bf16[4,16,2176]{2,1,0:T(8,128)(2,1)S(1)} %get-tuple-element.30), channel_id=1, source_target_pairs={{0,1},{1,0},{2,3},{3,2},{4,5},{5,4},{6,7},{7,6},{8,9},{9,8},{10,11... | collective-permute-start | bytes 835592 | tf_op jit(solution)/shard_map/ppermute | solution.py:346
  79.4 0.0 all-to-all-done.3.parts
  79.4 0.0 copy-done.1
  79.4 0.4 shard_map.150
  79.8 2.3 %all-gather.1 = bf16[8,16,2176]{2,1,0:T(8,128)(2,1)S(1)} all-gather(bf16[4,16,2176]{2,1,0:T(8,128)(2,1)S(1)} %get-tuple-element.28), channel_id=3, replica_groups=mesh['z'=8,'yy'=4,'hy'=2,'x'=4,'core'=2] {'core'}, dimensions={0}, use_global_device_ids=true | all-gather | bytes 835584 | tf_op jit(solution)/shard_map/all_gather | solution.py:363
  82.1 0.0 collective-permute-done.1.came_w
  82.1 0.3 shard_map.151
  82.4 0.0 copy-start.2
  82.4 12.8 %all_to_all.28.parts = bf16[4,16,4224]{2,1,0:T(8,128)(2,1)S(1)} all-to-all(bf16[4,16,4224]{2,1,0:T(8,128)(2,1)S(1)} %shard_map.151), channel_id=1, replica_groups=mesh['z'=8,'yy'=4,'hy'=2,'x'=4,'core'=2] {'x'}, dimensions={0} | all-to-all | bytes 1081344 | tf_op jit(solution)/shard_map/all_to_all | solution.py:301
  95.2 0.0 copy-done.2
  95.2 0.9 shard_map.152
  (2 shorter events, 0.0 us)
Async XLA Ops:
  36.6 18.2 %copy-start.3 = (f32[2]{0:T(128)S(1)}, f32[2]{0:T(128)}, u32[]{:S(2)}) copy-start(f32[2]{0:T(128)} %bias.1) | copy-start | bytes 28
  54.7 20.7 %copy-start = (bf16[128,2048]{1,0:T(8,128)(2,1)S(1)}, bf16[128,2048]{1,0:T(8,128)(2,1)}, u32[]{:S(2)}) copy-start(bf16[128,2048]{1,0:T(8,128)(2,1)} %w_out.2) | copy-start | bytes 1572868
  61.9 17.5 %copy-start.1 = (bf16[128,2048]{1,0:T(8,128)(2,1)S(1)}, bf16[128,2048]{1,0:T(8,128)(2,1)}, u32[]{:S(2)}) copy-start(bf16[128,2048]{1,0:T(8,128)(2,1)} %w_out.3) | copy-start | bytes 1572868
  61.9 17.5 %all-to-all-start.3 = ((bf16[16,72,128]{2,1,0:T(8,128)(2,1)}), bf16[16,72,128]{2,1,0:T(8,128)(2,1)S(1)}, u32[]{:S(2)}, u32[]{:S(2)}) async-start(bf16[16,72,128]{2,1,0:T(8,128)(2,1)} %shard_map.148), calls=%async_computation.3 | async-start | bytes 589824 | tf_op jit(solution)/shard_map/all_to_all | solution.py:301
  67.3 8.1 %collective-permute-start = (bf16[128,128]{1,0:T(8,128)(2,1)S(1)}, bf16[128,128]{1,0:T(8,128)(2,1)S(1)}, u32[]{:S(2)}, u32[]{:S(2)}) collective-permute-start(bf16[128,128]{1,0:T(8,128)(2,1)S(1)} %get-tuple-element.25.own), channel_id=1, source_target_pairs={{0,8},{8,16},{16,24},{24,32},{32,40},{40,48},{48,56},{56,64},{64,7... | collective-permute-start | bytes 98312 | tf_op jit(solution)/shard_map/ppermute | solution.py:336
  75.4 0.7 copy-start.4
  75.4 0.7 copy-start.5
  75.4 0.7 copy-start.6
  77.4 4.7 %collective-permute-start.1 = (bf16[4,16,2176]{2,1,0:T(8,128)(2,1)S(1)}, bf16[4,16,2176]{2,1,0:T(8,128)(2,1)S(1)}, u32[]{:S(2)}, u32[]{:S(2)}) collective-permute-start(bf16[4,16,2176]{2,1,0:T(8,128)(2,1)S(1)} %get-tuple-element.30), channel_id=1, source_target_pairs={{0,1},{1,0},{2,3},{3,2},{4,5},{5,4},{6,7},{7,6},{8,9},{9,8},{10,11... | collective-permute-start | bytes 835592 | tf_op jit(solution)/shard_map/ppermute | solution.py:346
  82.4 12.9 %copy-start.2 = (f32[2048]{0:T(1024)S(1)}, f32[2048]{0:T(1024)}, u32[]{:S(2)}) copy-start(f32[2048]{0:T(1024)} %param.29) | copy-start | bytes 24580
